TPU v7x, 32 devices: a whole 2x2x4 slice. The times are simulated.
32 devices in a mesh: fs: 16 (over z, y, x), tp: 2 (over core).
Axes of the slice: x: 2, y: 2, z: 4, core: 2. Of those that a mesh axis runs over, the one named last changes fastest.
Arguments:
- residual_in: bfloat16 [4096, 2048], P(('fs', 'tp')), may hold values from -6 to 6
- gain_first: float32 [2048], replicated, may hold values from 0.1 to 1.9
- gain_mixer: float32 [2048], replicated, may hold values from 0.1 to 1.9
- gain_second: float32 [2048], replicated, may hold values from 0.1 to 1.9
- gate_weight: float32 [2048, 6144], P('fs', 'tp'), may hold values from -0.125 to 0.125
- gate_scale: float32 [6144], P('tp'), may hold values from 0.3 to 3
- up_weight: float32 [2048, 6144], P('fs', 'tp'), may hold values from -0.125 to 0.125
- up_scale: float32 [6144], P('tp'), may hold values from 0.3 to 3
- down_weight: float32 [6144, 2048], P('tp', 'fs'), may hold values from -0.078125 to 0.078125
- down_scale: float32 [2048], P('fs'), may hold values from 0.3 to 3
- query_weight: float32 [2048, 2048], P('fs', 'tp'), may hold values from -0.125 to 0.125
- query_scale: float32 [2048], P('tp'), may hold values from 0.3 to 3
- key_weight: float32 [2048, 2048], P('fs', 'tp'), may hold values from -0.125 to 0.125
- key_scale: float32 [2048], P('tp'), may hold values from 0.3 to 3
- value_weight: float32 [2048, 2048], P('fs', 'tp'), may hold values from -0.125 to 0.125
- value_scale: float32 [2048], P('tp'), may hold values from 0.3 to 3
- output_weight: float32 [2048, 2048], P('tp', 'fs'), may hold values from -0.125 to 0.125
- output_scale: float32 [2048], P('fs'), may hold values from 0.3 to 3
Outputs:
- residual_out: bfloat16 [4096, 2048], P(('fs', 'tp'))
All inputs are finite; a program needn't handle non-finite values.
Results may differ from a plain program's by a relative error of at most 0.028.
Values may be sent and summed in bfloat16 or wider, within the bound.
A program may use at most 128 MiB of HBM per device.

v0:
```python
import math

import jax
import jax.numpy as jnp
from jax import lax
from jax.sharding import PartitionSpec as P

HEADS = 8
HEAD_DIM = 256
BLOCK = 64


EPSILON = 1e-06
HEAD_FLOOR = 0.25
ROTARY_BASE = 10000.0
HIGHEST = lax.Precision.HIGHEST


def normalize(sequence_rows, gain_vector):
    values = sequence_rows.astype(jnp.float32)
    scaled = values * lax.rsqrt(jnp.mean(values * values, axis=-1, keepdims=True) + EPSILON)
    return (scaled * gain_vector).astype(jnp.bfloat16)


def head_rates(first_head, head_count, length):
    head_number = (first_head + jnp.arange(head_count)).astype(jnp.float32)
    return jnp.exp(jnp.log(1.0 / 16.0) + head_number / (HEADS - 1) * jnp.log(4.0 / length))


def rotate(values, positions):
    half_width = values.shape[-1] // 2
    frequency = ROTARY_BASE ** (-jnp.arange(half_width, dtype=jnp.float32) * 2.0 / values.shape[-1])
    angles = positions[:, None] * frequency[None, :]
    cosine = jnp.cos(angles)[:, None, :]
    sine_value = jnp.sin(angles)[:, None, :]
    front_half = values[..., :half_width]
    back_half = values[..., half_width:]
    return jnp.concatenate(
        [
            front_half * cosine - back_half * sine_value,
            back_half * cosine + front_half * sine_value,
        ],
        axis=-1,
    )


def retention(query_pre, key_pre, value_pre, decay_rates):
    length, head_count, head_width = query_pre.shape
    positions = jnp.arange(length, dtype=jnp.float32)
    query_rot = rotate(query_pre, positions).astype(jnp.bfloat16)
    key_rot = rotate(key_pre, positions).astype(jnp.bfloat16)
    value_low = value_pre.astype(jnp.bfloat16)
    blocks = length // BLOCK
    inside = jnp.arange(BLOCK, dtype=jnp.float32)
    distance = inside[:, None] - inside[None, :]
    within = jnp.where(
        distance >= 0, jnp.exp(-decay_rates[:, None, None] * jnp.maximum(distance, 0.0)), 0.0
    ) * head_width ** (-0.5)
    query_blocks = query_rot.reshape(blocks, BLOCK, head_count, head_width)
    key_blocks = key_rot.reshape(blocks, BLOCK, head_count, head_width)
    value_blocks = value_low.reshape(blocks, BLOCK, head_count, head_width)
    scores = jnp.einsum(
        "nihe,njhe->nhij", query_blocks, key_blocks, preferred_element_type=jnp.float32
    )
    weights = (scores * within[None]).astype(jnp.bfloat16)
    inner_part = jnp.einsum(
        "nhij,njhe->nihe", weights, value_blocks, preferred_element_type=jnp.float32
    )
    fading = jnp.exp(-decay_rates[None, :] * (BLOCK - 1.0 - inside[:, None])) * head_width ** (-0.5)
    key_faded = key_blocks.astype(jnp.float32) * fading[None, :, :, None]
    updates = jnp.einsum(
        "njhd,njhe->nhde", key_faded, value_blocks.astype(jnp.float32), precision=HIGHEST
    )
    block_decay = jnp.exp(-decay_rates * BLOCK)

    def advance(memory_state, update):
        return (memory_state * block_decay[:, None, None] + update, memory_state)

    _, before = lax.scan(
        advance, jnp.zeros((head_count, head_width, head_width), jnp.float32), updates
    )
    rising = jnp.exp(-decay_rates[None, :] * (inside[:, None] + 1.0))
    queried = query_blocks.astype(jnp.float32) * rising[None, :, :, None]
    carried_part = jnp.einsum("nihd,nhde->nihe", queried, before, precision=HIGHEST)
    combined = (inner_part + carried_part).reshape(length, head_count, head_width)
    normed = combined * lax.rsqrt(
        jnp.maximum(jnp.mean(combined * combined, axis=-1, keepdims=True), HEAD_FLOOR)
    )
    return normed.astype(jnp.bfloat16).reshape(length, head_count * head_width)


def split_three(values):
    high = values.astype(jnp.bfloat16)
    rest = values - high.astype(jnp.float32)
    middle_part = rest.astype(jnp.bfloat16)
    low = (rest - middle_part.astype(jnp.float32)).astype(jnp.bfloat16)
    return [high, middle_part, low]


def make_body(n_fs, n_tp, share):
    spread = n_fs // share
    STRIDED = False
    if STRIDED:
        teams = [[m * spread + r for m in range(share)] for r in range(spread)]
    else:
        teams = [[r * share + m for m in range(share)] for r in range(spread)]
    twins = [[team[m] for team in teams] for m in range(share)]
    row_teams = [[f * n_tp + t for f in team for t in range(n_tp)] for team in teams]

    def my_rank():
        position = lax.axis_index("fs")
        return position // spread if STRIDED else position % share

    def fetch(pieces):
        swapped = lax.all_to_all(
            pieces, "fs", split_axis=0, concat_axis=0, axis_index_groups=teams, tiled=True
        )
        return lax.all_gather(swapped, "fs", axis=0, axis_index_groups=twins, tiled=False)

    def order_features(rows):
        if not STRIDED:
            return rows
        count = rows.shape[0]
        return rows.reshape(count, share, spread, -1).swapaxes(1, 2).reshape(count, -1)

    def collect_rows(rows, gain_vector):
        return lax.all_gather(
            order_features(normalize(rows, gain_vector)),
            ("fs", "tp"),
            axis=0,
            axis_index_groups=row_teams,
            tiled=True,
        )

    def return_rows(inputs, weight, factor):
        term = jnp.dot(inputs, weight, preferred_element_type=jnp.float32) * factor
        return lax.psum_scatter(
            term.astype(jnp.bfloat16),
            ("fs", "tp"),
            scatter_dimension=0,
            axis_index_groups=row_teams,
            tiled=True,
        ).astype(jnp.float32)

    def columns_of(weight):
        low = weight.astype(jnp.bfloat16)
        return low.reshape(low.shape[0], share, -1).swapaxes(0, 1)

    def rows_of(weight):
        low = weight.astype(jnp.bfloat16)
        return low.reshape(share, -1, low.shape[1])

    def own(vector, rank):
        width = vector.shape[0] // share
        return lax.dynamic_slice_in_dim(vector, rank * width, width)

    def body(
        residual_in,
        gain_first,
        gain_mixer,
        gain_second,
        gate_weight,
        gate_scale,
        up_weight,
        up_scale,
        down_weight,
        down_scale,
        query_weight,
        query_scale,
        key_weight,
        key_scale,
        value_weight,
        value_scale,
        output_weight,
        output_scale,
    ):
        rank = my_rank()
        hidden_width = gate_weight.shape[1] // share
        mix_width = query_weight.shape[1] // share
        entry = fetch(jnp.concatenate([columns_of(gate_weight), columns_of(up_weight)], axis=2))
        factors = split_three(down_scale) + split_three(output_scale)
        factors = jnp.stack(factors + [jnp.zeros_like(factors[0])] * 10)
        leave_piece = jnp.concatenate(
            [
                rows_of(down_weight),
                rows_of(output_weight),
                jnp.broadcast_to(factors[None], (share,) + factors.shape),
            ],
            axis=1,
        )
        first_input = collect_rows(residual_in, gain_first)
        leave_piece, entry = lax.optimization_barrier((leave_piece, entry)) if False else (leave_piece, entry)
        leave = fetch(leave_piece)
        project_piece = jnp.concatenate(
            [columns_of(query_weight), columns_of(key_weight), columns_of(value_weight)], axis=2
        )
        project_piece, leave = lax.optimization_barrier((project_piece, leave)) if False else (project_piece, leave)
        project = fetch(project_piece)

        entry = entry.reshape(-1, 2 * hidden_width)
        project = project.reshape(-1, 3 * mix_width)
        if STRIDED:
            leave = leave.swapaxes(0, 1)
        leave = leave.transpose(2, 0, 1, 3).reshape(leave.shape[2], -1)
        down_full = leave[:hidden_width]
        output_full = leave[hidden_width : hidden_width + mix_width]
        parts = leave[hidden_width + mix_width :].astype(jnp.float32)
        down_factor = parts[0] + parts[1] + parts[2]
        output_factor = parts[3] + parts[4] + parts[5]
        gate_own, up_own = own(gate_scale, rank), own(up_scale, rank)

        def half_step(inputs):
            both = jnp.dot(inputs, entry, preferred_element_type=jnp.float32)
            gate_pre = both[:, :hidden_width] * gate_own
            up_pre = both[:, hidden_width:] * up_own
            hidden = (jax.nn.silu(gate_pre) * up_pre).astype(jnp.bfloat16)
            return return_rows(hidden, down_full, down_factor)

        mlp_first = half_step(first_input)
        middle = (residual_in.astype(jnp.float32) + 0.5 * mlp_first).astype(jnp.bfloat16)
        mixer_input = collect_rows(middle, gain_mixer)
        both = jnp.dot(mixer_input, project, preferred_element_type=jnp.float32)
        scale = jnp.concatenate([own(v, rank) for v in (query_scale, key_scale, value_scale)])
        length = residual_in.shape[0] * n_tp
        heads_own = mix_width // HEAD_DIM
        both = (both * scale).reshape(share, length, 3, heads_own, HEAD_DIM)
        first_head = (lax.axis_index("tp") * share + rank) * heads_own
        decay_rates = head_rates(first_head, heads_own, length)
        mixed = jax.vmap(lambda t: retention(t[:, 0], t[:, 1], t[:, 2], decay_rates))(both)
        mixer_out = return_rows(mixed.reshape(share * length, mix_width), output_full, output_factor)
        second = (middle.astype(jnp.float32) + mixer_out).astype(jnp.bfloat16)
        mlp_second = half_step(collect_rows(second, gain_second))
        return (second.astype(jnp.float32) + 0.5 * mlp_second).astype(jnp.bfloat16)

    return body


def solution(mesh):
    n_fs, n_tp = mesh.shape["fs"], mesh.shape["tp"]
    share = math.gcd(math.gcd(HEADS // n_tp, n_fs), 4)
    body = make_body(n_fs, n_tp, share)
    in_specs = (
        P(("fs", "tp"), None),
        P(),
        P(),
        P(),
        P("fs", "tp"),
        P("tp"),
        P("fs", "tp"),
        P("tp"),
        P("tp", "fs"),
        P("fs"),
        P("fs", "tp"),
        P("tp"),
        P("fs", "tp"),
        P("tp"),
        P("fs", "tp"),
        P("tp"),
        P("tp", "fs"),
        P("fs"),
    )
    out_specs = P(("fs", "tp"), None)
    return jax.shard_map(body, mesh=mesh, in_specs=in_specs, out_specs=out_specs, check_vma=False)
```

profile of v0, /device:TPU:0, one launch (start us, length us, event | category | flops | bytes accessed | tf_op | source)
XLA Modules:
  0.0 651.8 jit_solution(6444827815063190604)
XLA Ops:
  9.3 19.7 %all_to_all.15 = bf16[4,1040,128]{2,1,0:T(8,128)(2,1)} all-to-all(bf16[4,1040,128]{2,1,0:T(8,128)(2,1)S(1)} %pad_maximum_fusion.1), channel_id=1, replica_groups={{0,2,4,6},{8,10,12,14},{16,18,20,22},{24,26,28,30},{1,3,5,7},{9,11,13,1..., dimensions={0} | all-to-all | bytes 2129920 | tf_op jit(solution)/shard_map/all_to_all | solution.py:115
  30.4 1.8 copy.71
  34.1 21.3 %all_to_all.16 = bf16[4,128,1536]{1,2,0:T(8,128)(2,1)S(1)} all-to-all(bf16[4,128,1536]{1,2,0:T(8,128)(2,1)S(1)} %pad_maximum_fusion), channel_id=1, replica_groups={{0,2,4,6},{8,10,12,14},{16,18,20,22},{24,26,28,30},{1,3,5,7},{9,11,13,1..., dimensions={0} | all-to-all | bytes 3145728 | tf_op jit(solution)/shard_map/all_to_all | solution.py:115
  58.6 51.9 %all-gather.18.cloned.1.call-done = bf16[16,1040,128]{2,1,0:T(8,128)(2,1)} async-done(((bf16[4,1040,128]{2,1,0:T(8,128)(2,1)}), bf16[16,1040,128]{2,1,0:T(8,128)(2,1)}) %all-gather.18.cloned.1.call-update) | async-done | bytes 4259856 | tf_op jit(solution)/shard_map/all_gather | solution.py:118
  110.5 6.4 copy.74
  116.9 4.1 slice.98
  122.1 2.0 fusion.35
  124.2 23.3 %all-gather.10.cloned.1.call-done = bf16[1024,2048]{1,0:T(8,128)(2,1)} async-done(((bf16[128,2048]{1,0:T(8,128)(2,1)}), bf16[1024,2048]{1,0:T(8,128)(2,1)}) %all-gather.10.cloned.1.call-update) | async-done | bytes 4194320 | tf_op jit(solution)/shard_map/all_gather | solution.py:127
  147.5 116.9 %all-gather.16.cloned.1.call-done = bf16[16,128,1536]{2,1,0:T(8,128)(2,1)} async-done(((bf16[4,128,1536]{2,1,0:T(8,128)(2,1)}), bf16[16,128,1536]{2,1,0:T(8,128)(2,1)}) %all-gather.16.cloned.1.call-update) | async-done | bytes 6291472 | tf_op jit(solution)/shard_map/all_gather | solution.py:118
  264.4 10.1 %fusion.54 = f32[1024,1536]{1,0:T(8,128)S(1)} fusion(bf16[1024,2048]{1,0:T(8,128)(2,1)} %all-gather.10.cloned.1.call-done, bf16[2048,1536]{1,0:T(8,128)(2,1)} %bitcast.133), kind=kOutput, calls=%fused_computation.106 | convolution fusion | flops 6442450944 | bytes 16777216 | tf_op jit(solution)/shard_map/dot_general | solution.py:213
  274.6 5.1 multiply_convert_fusion.2
  281.3 15.0 %all_to_all.17 = bf16[4,128,768]{1,2,0:T(8,128)(2,1)S(1)} all-to-all(bf16[4,128,768]{1,2,0:T(8,128)(2,1)S(1)} %pad_maximum_fusion.2), channel_id=1, replica_groups={{0,2,4,6},{8,10,12,14},{16,18,20,22},{24,26,28,30},{1,3,5,7},{9,11,13,1..., dimensions={0} | all-to-all | bytes 1572864 | tf_op jit(solution)/shard_map/all_to_all | solution.py:115
  297.5 31.7 %reduce-scatter.4.cloned.1.call-done = bf16[128,2048]{1,0:T(8,128)(2,1)} async-done(((bf16[1024,2048]{1,0:T(8,128)(2,1)}), bf16[128,2048]{1,0:T(8,128)(2,1)}) %reduce-scatter.4.cloned.1.call-update) | async-done | bytes 524304 | tf_op jit(solution)/shard_map/reduce_scatter | solution.py:137
  336.6 2.4 slice.110
  339.0 55.1 %all-gather.20.cloned.1.call-done = bf16[16,128,768]{2,1,0:T(8,128)(2,1)} async-done(((bf16[4,128,768]{2,1,0:T(8,128)(2,1)}), bf16[16,128,768]{2,1,0:T(8,128)(2,1)}) %all-gather.20.cloned.1.call-update) | async-done | bytes 3145744 | tf_op jit(solution)/shard_map/all_gather | solution.py:118
  394.1 37.0 %all-gather.12.cloned.1.call-done = bf16[1024,2048]{1,0:T(8,128)(2,1)} async-done(((bf16[128,2048]{1,0:T(8,128)(2,1)}), bf16[1024,2048]{1,0:T(8,128)(2,1)}) %all-gather.12.cloned.1.call-update) | async-done | bytes 4194320 | tf_op jit(solution)/shard_map/all_gather | solution.py:127
  431.1 8.3 %convolution_multiply_fusion = f32[1024,768]{1,0:T(8,128)} fusion(bf16[1024,2048]{1,0:T(8,128)(2,1)} %all-gather.12.cloned.1.call-done, bf16[2048,768]{1,0:T(8,128)(2,1)} %bitcast.135, f32[768]{0:T(1024)S(1)} %pad_maximum_fusion.11), kind=kOutput, calls=%fused_computation.18 | convolution fusion | flops 3222011904 | bytes 10488832 | tf_op jit(solution)/shard_map/dot_general | solution.py:222
  439.4 3.5 copy.79
  442.9 5.2 reshape.332
  448.2 2.2 slice.162
  454.5 2.4 subtract_convert_fusion.1
  460.6 4.7 convolution_bitcast_fusion
  465.3 10.6 %while.13 = (s32[]{:T(128)}, f32[4,1,256,256]{3,2,1,0:T(8,128)S(1)}, f32[4,4,1,256,256]{4,3,1,2,0:T(8,128)}, f32[1]{0:T(128)}, f32[4,4,1,256,256]{4,3,0,1,2:T(8,128)}, /*index=5*/s32[]{:T(128)}, s32[]{:T(128)}) while((s32[]{:T(128)}, f32[4,1,256,256]{3,2,1,0:T(8,128)S(1)}, f32[4,4,1,256,256]{4,3,1,2,0:T(8,128)}, f32[1]{0:T(128)}, ...), condition=%wide.region_4.5_spmd.clone, body=%wide.region_3.4_spmd.clone.sunk | while | flops 1048579 | bytes 5242988 | solution.py:79
  476.3 5.2 multiply_reduce_fusion
  481.8 3.4 multiply_convert_fusion.1
  485.2 51.2 %reduce-scatter.6.cloned.1.call-done = bf16[128,2048]{1,0:T(8,128)(2,1)} async-done(((bf16[1024,2048]{1,0:T(8,128)(2,1)}), bf16[128,2048]{1,0:T(8,128)(2,1)}) %reduce-scatter.6.cloned.1.call-update) | async-done | bytes 524304 | tf_op jit(solution)/shard_map/reduce_scatter | solution.py:137
  537.8 2.0 fusion.33
  539.9 36.7 %all-gather.14.cloned.1.call-done = bf16[1024,2048]{1,0:T(8,128)(2,1)} async-done(((bf16[128,2048]{1,0:T(8,128)(2,1)}), bf16[1024,2048]{1,0:T(8,128)(2,1)}) %all-gather.14.cloned.1.call-update) | async-done | bytes 4194320 | tf_op jit(solution)/shard_map/all_gather | solution.py:127
  576.6 10.1 %fusion.55 = f32[1024,1536]{1,0:T(8,128)S(1)} fusion(bf16[1024,2048]{1,0:T(8,128)(2,1)} %all-gather.14.cloned.1.call-done, bf16[2048,1536]{1,0:T(8,128)(2,1)} %bitcast.134), kind=kOutput, calls=%fused_computation.107 | convolution fusion | flops 6442450944 | bytes 16777216 | tf_op jit(solution)/shard_map/dot_general | solution.py:213
  586.8 5.1 multiply_convert_fusion
  591.9 51.3 %reduce-scatter.8.cloned.1.call-done = bf16[128,2048]{1,0:T(8,128)(2,1)} async-done(((bf16[1024,2048]{1,0:T(8,128)(2,1)}), bf16[128,2048]{1,0:T(8,128)(2,1)}) %reduce-scatter.8.cloned.1.call-update) | async-done | bytes 524304 | tf_op jit(solution)/shard_map/reduce_scatter | solution.py:137
  643.2 2.1 fusion.34
  (111 shorter events, 40.8 us)
Async XLA Ops:
  6.5 2.6 copy-start.17
  6.5 2.6 copy-start.18
  6.5 103.9 %all-gather.18.cloned.1.call-start = ((), (), s32[]{:S(2)}) async-start(), calls=%async_computation.13 | async-start | bytes 5324800 | tf_op jit(solution)/shard_map/all_gather | solution.py:118
  9.1 20.0 %copy-start = (bf16[128,2048]{1,0:T(8,128)(2,1)S(1)}, bf16[128,2048]{1,0:T(8,128)(2,1)}, u32[]{:S(2)}) copy-start(bf16[128,2048]{1,0:T(8,128)(2,1)} %param.20) | copy-start | bytes 1572868
  9.2 20.2 %copy-start.9 = (f32[2048]{0:T(1024)S(1)}, f32[2048]{0:T(1024)}, u32[]{:S(2)}) copy-start(f32[2048]{0:T(1024)} %param.21) | copy-start | bytes 24580
  29.1 118.4 %all-gather.10.cloned.1.call-start = ((), (), s32[]{:S(2)}) async-start(), calls=%async_computation.6 | async-start | bytes 4718592 | tf_op jit(solution)/shard_map/all_gather | solution.py:127
  30.4 234.0 %all-gather.16.cloned.1.call-start = ((), (), s32[]{:S(2)}) async-start(), calls=%async_computation.12 | async-start | bytes 7864320 | tf_op jit(solution)/shard_map/all_gather | solution.py:118
  57.0 272.2 %reduce-scatter.4.cloned.1.call-start = ((), (), s32[]{:S(2)}) async-start(), calls=%async_computation.7 | async-start | bytes 4718592 | tf_op jit(solution)/shard_map/reduce_scatter | solution.py:137
  57.8 216.7 %copy-start.12 = (f32[768]{0:T(1024)}, f32[768]{0:T(1024)S(1)}, u32[]{:S(2)}) copy-start(f32[768]{0:T(1024)S(1)} %dynamic_slice.19) | copy-start | bytes 9220
  58.6 215.9 %copy-start.14 = (f32[768]{0:T(1024)}, f32[768]{0:T(1024)S(1)}, u32[]{:S(2)}) copy-start(f32[768]{0:T(1024)S(1)} %dynamic_slice.20) | copy-start | bytes 9220
  264.4 10.2 %copy-start.2 = (bf16[768,4,4,128]{0,3,2,1:T(8,128)(2,1)S(1)}, bf16[768,4,4,128]{0,3,2,1:T(8,128)(2,1)}, u32[]{:S(2)}) copy-start(bf16[768,4,4,128]{0,3,2,1:T(8,128)(2,1)} %slice.98) | copy-start | bytes 9437188
  279.7 1.0 copy-start.5
  279.7 1.2 copy-start.6
  279.7 1.4 copy-start.7
  279.7 114.4 %all-gather.20.cloned.1.call-start = ((), (), s32[]{:S(2)}) async-start(), calls=%async_computation.14 | async-start | bytes 3932160 | tf_op jit(solution)/shard_map/all_gather | solution.py:118
  281.3 49.3 %copy-start.10 = (f32[2048]{0:T(1024)S(1)}, f32[2048]{0:T(1024)}, u32[]{:S(2)}) copy-start(f32[2048]{0:T(1024)} %param.22) | copy-start | bytes 24580
  297.5 133.6 %all-gather.12.cloned.1.call-start = ((), (), s32[]{:S(2)}) async-start(), calls=%async_computation.8 | async-start | bytes 4718592 | tf_op jit(solution)/shard_map/all_gather | solution.py:127
  331.6 204.9 %reduce-scatter.6.cloned.1.call-start = ((), (), s32[]{:S(2)}) async-start(), calls=%async_computation.9 | async-start | bytes 4718592 | tf_op jit(solution)/shard_map/reduce_scatter | solution.py:137
  465.2 10.6 %copy-start.8 = (f32[64,64]{1,0:T(8,128)S(1)}, f32[64,64]{1,0:T(8,128)}, u32[]{:S(2)}) copy-start(f32[64,64]{1,0:T(8,128)} %select_multiply_fusion) | copy-start | bytes 49156
  465.3 11.1 %copy-start.16 = (f32[64]{0:T(128)S(1)}, f32[64]{0:T(128)}, u32[]{:S(2)}) copy-start(f32[64]{0:T(128)} %get-tuple-element.124) | copy-start | bytes 772
  476.3 5.5 copy-start.4
  485.2 52.6 %copy-start.11 = (f32[2048]{0:T(1024)S(1)}, f32[2048]{0:T(1024)}, u32[]{:S(2)}) copy-start(f32[2048]{0:T(1024)} %param.23) | copy-start | bytes 24580
  485.2 91.4 %all-gather.14.cloned.1.call-start = ((), (), s32[]{:S(2)}) async-start(), calls=%async_computation.10 | async-start | bytes 4718592 | tf_op jit(solution)/shard_map/all_gather | solution.py:127
  539.9 46.9 %copy-start.13 = (f32[768]{0:T(1024)S(1)}, f32[768]{0:T(1024)}, u32[]{:S(2)}) copy-start(f32[768]{0:T(1024)} %copy-done.12) | copy-start | bytes 9220
  539.9 46.9 %copy-start.15 = (f32[768]{0:T(1024)S(1)}, f32[768]{0:T(1024)}, u32[]{:S(2)}) copy-start(f32[768]{0:T(1024)} %copy-done.14) | copy-start | bytes 9220
  539.9 103.3 %reduce-scatter.8.cloned.1.call-start = ((), (), s32[]{:S(2)}) async-start(), calls=%async_computation.11 | async-start | bytes 4718592 | tf_op jit(solution)/shard_map/reduce_scatter | solution.py:137
  576.6 10.2 %copy-start.3 = (bf16[768,4,4,128]{0,3,2,1:T(8,128)(2,1)S(1)}, bf16[768,4,4,128]{0,3,2,1:T(8,128)(2,1)}, u32[]{:S(2)}) copy-start(bf16[768,4,4,128]{0,3,2,1:T(8,128)(2,1)} %slice.98) | copy-start | bytes 9437188
  591.9 51.3 %copy-start.1 = (bf16[128,2048]{1,0:T(8,128)(2,1)S(1)}, bf16[128,2048]{1,0:T(8,128)(2,1)}, u32[]{:S(2)}) copy-start(bf16[128,2048]{1,0:T(8,128)(2,1)} %reduce-scatter.6.cloned.1.call-done) | copy-start | bytes 1572868
Sparse Core Ops, SparseCore 0:
  29.2 81.2 all-gather.17
  112.4 35.0 all-gather.9
  149.0 115.3 all-gather.15
  279.8 49.3 reduce-scatter.3
  330.6 63.4 all-gather.19
  395.8 35.2 all-gather.11
  485.3 51.1 reduce-scatter.5
  540.0 36.5 all-gather.13
  592.0 51.1 reduce-scatter.7
where the time goes:
time: 653 us; the launch traced here: 652 us
  waiting for transfers between devices  455 us (70%)
  blocking collectives  56 us (9%)
  matrix products  52.5 us (8%)
  local copies, waits for them, and re-layouts  43.4 us (7%)
  other arithmetic  30.5 us (5%)
  between operations  13.7 us (2%)
    all_gather x3, waiting for transfers between devices, fetch(): lax.all_gather(swapped, 'fs', axis=0, axis_index_groups=twins, tiled=False)  224 us
    reduce_scatter x3, waiting for transfers between devices, return_rows(): lax.psum_scatter(term.astype(jnp.bfloat16), ('fs', 'tp'), scatter_dimensi...  134 us
    all_gather x3, waiting for transfers between devices, collect_rows(): lax.all_gather(order_features(normalize(rows, gain_vector)), ('fs', 'tp')...  96.9 us
    all_to_all x3, blocking collectives, fetch(): lax.all_to_all(pieces, 'fs', split_axis=0, concat_axis=0, axis_index_grou...  56 us
    dot_general x2, matrix products, half_step(): both = jnp.dot(inputs, entry, preferred_element_type=jnp.float32)  20.3 us
    dot_general x3, matrix products, return_rows(): term = jnp.dot(inputs, weight, preferred_element_type=jnp.float32) * factor  13.6 us
  transfers between devices with their start and end apart: 9, of which 9 were waited for; matrix products, arithmetic and copies ran while one was open for 5% of the time, Pallas kernels for 0%

commit v1 on v0

--- a/solution.py
+++ b/solution.py
@@ -1,8 +1,12 @@
+import functools
 import math
 
 import jax
 import jax.numpy as jnp
+import numpy as np
 from jax import lax
+from jax.experimental import pallas as pl
+from jax.experimental.pallas import tpu as pltpu
 from jax.sharding import PartitionSpec as P
 
 HEADS = 8
@@ -235,10 +239,407 @@
     return body
 
 
+MESH = pl.DeviceIdType.MESH
+GU, DN, QKV, OUT, SC = range(5)
+FAR_FIRST = ((1, 0, 0), (1, 1, 0), (1, 0, 1), (1, 1, 1), (0, 1, 0), (0, 1, 1), (0, 0, 1))
+TEAM = ((1, 1), (1, 0), (0, 1))
+LAG_REDUCE, LAG_FINISH, LAG_PASS = 1, 3, 5
+
+
+def fused_kernel(
+    res_ref, g1_ref, g2_ref, g3_ref,
+    gate_ref, up_ref, down_ref, q_ref, k_ref, v_ref, o_ref,
+    gs_ref, us_ref, qs_ref, ks_ref, vs_ref, scales_ref, cos_ref, sin_ref,
+    out_ref,
+    rows_raw, rows_normed, w_gu, w_d, w_qkv, w_o, w_sc,
+    st_gu, st_d, st_qkv, st_o, acc, hidden, mixed, part, part_twin, chip_part, far_part,
+    w_recv, w_send, w_fwd, ag_recv, ag_send, tw_recv, tw_send, rs_recv, rs_send,
+):
+    f32, bf16 = jnp.float32, jnp.bfloat16
+    f, t = lax.axis_index("fs"), lax.axis_index("tp")
+    x, y, z = f % 2, (f // 2) % 2, f // 4
+    zl, zh = z % 2, z // 2
+    me = zl * 2 + x
+    own = res_ref.shape[0]
+    width = res_ref.shape[1]
+    seq = 2 * own
+    ff = hidden.shape[1]
+    hd = mixed.shape[1]
+    piece = gate_ref.shape[0]
+    chunk = 2 * piece
+    chunks = width // chunk
+    f_y = z * 4 + (1 - y) * 2 + x
+
+    def plane_peer(dh, dl, dx):
+        hh, ll, xx = (zh + dh) % 2, (zl + dl) % 2, (x + dx) % 2
+        return (2 * hh + ll) * 4 + y * 2 + xx, ll * 2 + xx
+
+    def remote(src, dst, send, recv, fs, tp):
+        return pltpu.make_async_remote_copy(
+            src_ref=src, dst_ref=dst, send_sem=send, recv_sem=recv, device_id=(fs, tp), device_id_type=MESH
+        )
+
+    barrier = pltpu.get_barrier_semaphore()
+    for dh, dl, dx in FAR_FIRST:
+        peer, _ = plane_peer(dh, dl, dx)
+        pl.semaphore_signal(barrier, inc=1, device_id=(peer, t), device_id_type=MESH)
+    pl.semaphore_signal(barrier, inc=1, device_id=(f_y, t), device_id_type=MESH)
+    pl.semaphore_signal(barrier, inc=1, device_id=(f, 1 - t), device_id_type=MESH)
+    pl.semaphore_wait(barrier, 9)
+
+    def slot(kind, s):
+        if kind == GU:
+            return w_gu.at[pl.ds(pl.multiple_of(s * piece, piece), piece), :]
+        if kind == DN:
+            return w_d.at[:, pl.ds(pl.multiple_of(s * piece, piece), piece)]
+        if kind == QKV:
+            return w_qkv.at[pl.ds(pl.multiple_of(s * piece, piece), piece), :]
+        if kind == OUT:
+            return w_o.at[:, pl.ds(pl.multiple_of(s * piece, piece), piece)]
+        return w_sc.at[pl.ds(pl.multiple_of(s * 8, 8), 8), :]
+
+    def staged(kind, m):
+        if kind == SC:
+            return scales_ref
+        return {GU: st_gu, DN: st_d, QKV: st_qkv, OUT: st_o}[kind].at[m]
+
+    def send_pieces(kind):
+        remote(staged(kind, me), slot(kind, f), w_fwd.at[kind, me], w_recv.at[kind, f], f_y, t).start()
+        for i, (dh, dl, dx) in enumerate(FAR_FIRST):
+            peer, m = plane_peer(dh, dl, dx)
+            remote(staged(kind, m), slot(kind, f), w_send.at[kind, i], w_recv.at[kind, f], peer, t).start()
+        slot(kind, f)[...] = staged(kind, me)[...]
+
+    def pair_base(j):
+        zz = 2 * ((zh + (j // 2) % 2) % 2) + j % 2
+        return zz * 4 + ((y + j // 4) % 2) * 2
+
+    def take_pair(kind, j):
+        base = pair_base(j)
+        for xx in (0, 1):
+            s = base + xx
+
+            @pl.when(s != f)
+            def _():
+                remote(slot(kind, s), slot(kind, s), w_fwd.at[kind, 0], w_recv.at[kind, s], f_y, t).wait_recv()
+
+            @pl.when((s != f) & (j < 4))
+            def _():
+                remote(
+                    slot(kind, s), slot(kind, s), w_fwd.at[kind, (j % 4) * 2 + xx], w_recv.at[kind, s], f_y, t
+                ).start()
+
+    def take_all(kind):
+        def step(j, _):
+            take_pair(kind, j)
+            return 0
+
+        lax.fori_loop(0, 8, step, 0)
+
+    def finish_sends(kind):
+        for i, (dh, dl, dx) in enumerate(FAR_FIRST):
+            peer, m = plane_peer(dh, dl, dx)
+            remote(staged(kind, m), slot(kind, f), w_send.at[kind, i], w_recv.at[kind, f], peer, t).wait_send()
+        for i in range(8):
+            remote(slot(kind, f), slot(kind, f), w_fwd.at[kind, i], w_recv.at[kind, f], f_y, t).wait_send()
+
+    def block_rows(m, core):
+        return pl.ds(pl.multiple_of((m * 2 + core) * own, own), own)
+
+    def column(j):
+        return pl.multiple_of(pair_base(j) * piece, chunk)
+
+    def ag_copy(j, i, src, m, core, fs, tp):
+        dst = rows_raw.at[block_rows(m, core), pl.ds(column(j), chunk)]
+        return remote(dst if src is None else src, dst, ag_send.at[j, i], ag_recv.at[j, m * 2 + core], fs, tp)
+
+    def ag_start(j, src):
+        for i, (dl, dx) in enumerate(TEAM):
+            peer, _ = plane_peer(0, dl, dx)
+            ag_copy(j, i, src, me, t, peer, t).start()
+        ag_copy(j, 3, src, me, t, f, 1 - t).start()
+
+    def ag_pass(j):
+        for i, (dl, dx) in enumerate(TEAM):
+            _, m = plane_peer(0, dl, dx)
+            ag_copy(j, 4 + i, None, m, t, f, 1 - t).wait_recv()
+            ag_copy(j, 4 + i, None, m, t, f, 1 - t).start()
+
+    def ag_finish():
+        def step(j, _):
+            for m in range(4):
+                ag_copy(j, 0, None, m, 1 - t, f, 1 - t).wait_recv()
+            for i in range(7):
+                ag_copy(j, i, None, me, t, f, 1 - t).wait_send()
+            return 0
+
+        lax.fori_loop(0, chunks, step, 0)
+
+    def norm_rows(gain_ref):
+        def step(i, _):
+            at = pl.ds(pl.multiple_of(i * 32, 32), 32)
+            v = rows_raw[at, :].astype(f32)
+            r = lax.rsqrt(jnp.mean(v * v, axis=-1, keepdims=True) + EPSILON)
+            rows_normed[at, :] = (v * r * gain_ref[...]).astype(bf16)
+            return 0
+
+        lax.fori_loop(0, rows_raw.shape[0] // 32, step, 0)
+
+    def row_tiles(size, body):
+        def step(i, _):
+            body(pl.ds(pl.multiple_of(i * size, size), size))
+            return 0
+
+        lax.fori_loop(0, rows_raw.shape[0] // size, step, 0)
+
+    def accumulate(kind, weights, columns):
+        def step(j, _):
+            take_pair(kind, j)
+            at = pl.ds(column(j), chunk)
+
+            def tile(r):
+                acc[r, :columns] += jnp.dot(rows_normed[r, at], weights[at, :], preferred_element_type=f32)
+
+            row_tiles(seq, tile)
+            return 0
+
+        def clear(r):
+            acc[r, :columns] = jnp.zeros((seq, columns), f32)
+
+        row_tiles(seq, clear)
+        lax.fori_loop(0, 8, step, 0)
+
+    def silu_mul(gate, up):
+        gate = gate * gs_ref[...]
+        return (gate / (1.0 + jnp.exp(-gate)) * (up * us_ref[...])).astype(bf16)
+
+    def leave(inputs, weights, scale_row, factor, arriving, last):
+        def product(j):
+            if arriving is not None:
+                take_pair(arriving, j)
+            base = pair_base(j)
+            at = pl.ds(column(j), chunk)
+            factors = jnp.concatenate(
+                [w_sc[pl.ds((base + h) * 8 + scale_row, 1), :] for h in (0, 1)], axis=1
+            )
+
+            def step(m, _):
+                r = pl.ds(pl.multiple_of(m * seq, seq), seq)
+                term = jnp.dot(inputs[r, :], weights[:, at], preferred_element_type=f32) * factors
+                term = term.astype(bf16)
+                part[0, m, :, at] = term[:own]
+                part[1, m, :, at] = term[own:]
+                return 0
+
+            lax.fori_loop(0, 4, step, 0)
+            to_twin(j).start()
+
+        def to_twin(j):
+            at = pl.ds(column(j), chunk)
+            return remote(part.at[1 - t, :, :, at], part_twin.at[:, :, at], tw_send.at[j], tw_recv.at[j], f, 1 - t)
+
+        def to_team(j, i):
+            dl, dx = TEAM[i]
+            at = pl.ds(column(j), chunk)
+            peer, _ = plane_peer(0, dl, dx)
+            return remote(chip_part.at[i, :, at], far_part.at[i, :, at], rs_send.at[j, i], rs_recv.at[j, i], peer, t)
+
+        def reduce(j):
+            at = pl.ds(column(j), chunk)
+            to_twin(j).wait_recv()
+            for i, (dl, dx) in enumerate(TEAM):
+                _, m = plane_peer(0, dl, dx)
+                chip_part[i, :, at] = (part[t, m, :, at].astype(f32) + part_twin[m, :, at].astype(f32)).astype(bf16)
+                to_team(j, i).start()
+
+        def finish(j):
+            at = pl.ds(column(j), chunk)
+            total = part[t, me, :, at].astype(f32) + part_twin[me, :, at].astype(f32)
+            for i in range(3):
+                to_team(j, i).wait_recv()
+                total = total + far_part[i, :, at].astype(f32)
+            mine = block_rows(me, t)
+            fresh = (rows_raw[mine, at].astype(f32) + factor * total).astype(bf16)
+            if last:
+                out_ref[:, at] = fresh
+            else:
+                rows_raw[mine, at] = fresh
+                ag_start(j, None)
+
+        def step(i, _):
+            pl.when(i < chunks)(lambda: product(i))
+            j_reduce, j_finish, j_pass = i - LAG_REDUCE, i - LAG_FINISH, i - LAG_PASS
+            pl.when((j_reduce >= 0) & (j_reduce < chunks))(lambda: reduce(j_reduce))
+            pl.when((j_finish >= 0) & (j_finish < chunks))(lambda: finish(j_finish))
+            if not last:
+                pl.when(j_pass >= 0)(lambda: ag_pass(j_pass))
+            return 0
+
+        lax.fori_loop(0, chunks + (LAG_FINISH if last else LAG_PASS), step, 0)
+
+        def drain(j, _):
+            to_twin(j).wait_send()
+            for i in range(3):
+                to_team(j, i).wait_send()
+            return 0
+
+        lax.fori_loop(0, chunks, drain, 0)
+        if not last:
+            ag_finish()
+
+    def first_rows(j, _):
+        ag_start(j, res_ref.at[:, pl.ds(column(j), chunk)])
+        return 0
+
+    lax.fori_loop(0, chunks, first_rows, 0)
+    rows_raw[block_rows(me, t), :] = res_ref[...]
+
+    send_pieces(SC)
+    for m in range(4):
+        at = slice(m * ff, (m + 1) * ff)
+        st_gu[m, :, :ff] = gate_ref[:, at].astype(bf16)
+        st_gu[m, :, ff:] = up_ref[:, at].astype(bf16)
+    send_pieces(GU)
+    for m in range(4):
+        st_d[m] = down_ref[m * ff : (m + 1) * ff, :].astype(bf16)
+    send_pieces(DN)
+    for m in range(4):
+        at = slice(m * hd, (m + 1) * hd)
+        st_qkv[m, :, :hd] = q_ref[:, at].astype(bf16)
+        st_qkv[m, :, hd : 2 * hd] = k_ref[:, at].astype(bf16)
+        st_qkv[m, :, 2 * hd :] = v_ref[:, at].astype(bf16)
+        st_o[m] = o_ref[at, :].astype(bf16)
+    send_pieces(QKV)
+    send_pieces(OUT)
+
+    def first_pass(j, _):
+        ag_pass(j)
+        return 0
+
+    lax.fori_loop(0, chunks, first_pass, 0)
+    ag_finish()
+    norm_rows(g1_ref)
+    take_all(SC)
+
+    accumulate(GU, w_gu, 2 * ff)
+
+    def first_hidden(r):
+        hidden[r, :] = silu_mul(acc[r, :ff], acc[r, ff:])
+
+    row_tiles(own, first_hidden)
+    leave(hidden, w_d, 0, 0.5, DN, False)
+
+    norm_rows(g2_ref)
+    accumulate(QKV, w_qkv, 3 * hd)
+    take_all(OUT)
+    head = (t * 4 + me).astype(f32)
+    ri = lax.broadcasted_iota(jnp.int32, (seq, seq), 0)
+    ci = lax.broadcasted_iota(jnp.int32, (seq, seq), 1)
+    rate = jnp.exp(math.log(1.0 / 16.0) + jnp.full((seq, seq), head, f32) / (HEADS - 1) * math.log(4.0 / seq))
+    distance = jnp.maximum(ri - ci, 0).astype(f32)
+    decay = jnp.where(ri >= ci, jnp.exp(-rate * distance), 0.0) * hd ** (-0.5)
+
+    def turn(values):
+        a, b = values[:, : hd // 2], values[:, hd // 2 :]
+        c, s = cos_ref[...], sin_ref[...]
+        return jnp.concatenate([a * c - b * s, b * c + a * s], axis=1).astype(bf16)
+
+    def sequence(r):
+        q = turn(acc[r, :hd] * qs_ref[...])
+        k = turn(acc[r, hd : 2 * hd] * ks_ref[...])
+        v = (acc[r, 2 * hd : 3 * hd] * vs_ref[...]).astype(bf16)
+        scores = lax.dot_general(q, k, (((1,), (1,)), ((), ())), preferred_element_type=f32)
+        both = jnp.dot((scores * decay).astype(bf16), v, preferred_element_type=f32)
+        level = jnp.maximum(jnp.mean(both * both, axis=-1, keepdims=True), HEAD_FLOOR)
+        mixed[r, :] = (both * lax.rsqrt(level)).astype(bf16)
+
+    row_tiles(seq, sequence)
+    leave(mixed, w_o, 1, 1.0, None, False)
+
+    norm_rows(g3_ref)
+
+    def second_hidden(r):
+        gate = jnp.dot(rows_normed[r, :], w_gu[:, :ff], preferred_element_type=f32)
+        up = jnp.dot(rows_normed[r, :], w_gu[:, ff:], preferred_element_type=f32)
+        hidden[r, :] = silu_mul(gate, up)
+
+    row_tiles(seq, second_hidden)
+    leave(hidden, w_d, 0, 0.5, None, True)
+    for kind in (SC, GU, DN, QKV, OUT):
+        finish_sends(kind)
+
+
+def fused_body(
+    residual_in, gain_first, gain_mixer, gain_second,
+    gate_weight, gate_scale, up_weight, up_scale, down_weight, down_scale,
+    query_weight, query_scale, key_weight, key_scale, value_weight, value_scale,
+    output_weight, output_scale,
+):
+    f32, bf16 = jnp.float32, jnp.bfloat16
+    own, width = residual_in.shape
+    rows, piece = 8 * own, gate_weight.shape[0]
+    ff, hd = gate_weight.shape[1] // 4, query_weight.shape[1] // 4
+    chunks = width // (2 * piece)
+    x, z = lax.axis_index("fs") % 2, lax.axis_index("fs") // 4
+    me = (z % 2) * 2 + x
+
+    def part_of(vector, size):
+        return lax.dynamic_slice_in_dim(vector, me * size, size).reshape(1, -1)
+
+    scales = jnp.concatenate([down_scale[None], output_scale[None], jnp.zeros((6, piece), f32)])
+    half = hd // 2
+    frequency = np.float32(ROTARY_BASE) ** (-np.arange(half, dtype=np.float32) * np.float32(2.0) / np.float32(hd))
+    angles = np.arange(2 * own, dtype=np.float32)[:, None] * frequency.astype(np.float32)[None]
+    cosine, sine_value = np.cos(angles).astype(np.float32), np.sin(angles).astype(np.float32)
+    operands = (
+        residual_in, gain_first.reshape(1, -1), gain_mixer.reshape(1, -1), gain_second.reshape(1, -1),
+        gate_weight, up_weight, down_weight, query_weight, key_weight, value_weight, output_weight,
+        part_of(gate_scale, ff), part_of(up_scale, ff),
+        part_of(query_scale, hd), part_of(key_scale, hd), part_of(value_scale, hd),
+        scales, jnp.asarray(cosine), jnp.asarray(sine_value),
+    )
+    dma = pltpu.SemaphoreType.DMA
+    return pl.pallas_call(
+        fused_kernel,
+        out_shape=jax.ShapeDtypeStruct((own, width), bf16),
+        in_specs=[pl.BlockSpec(memory_space=pltpu.VMEM)] * len(operands),
+        out_specs=pl.BlockSpec(memory_space=pltpu.VMEM),
+        scratch_shapes=[
+            pltpu.VMEM((rows, width), bf16),
+            pltpu.VMEM((rows, width), bf16),
+            pltpu.VMEM((width, 2 * ff), bf16),
+            pltpu.VMEM((ff, width), bf16),
+            pltpu.VMEM((width, 3 * hd), bf16),
+            pltpu.VMEM((hd, width), bf16),
+            pltpu.VMEM((8 * (width // piece), piece), f32),
+            pltpu.VMEM((4, piece, 2 * ff), bf16),
+            pltpu.VMEM((4, ff, piece), bf16),
+            pltpu.VMEM((4, piece, 3 * hd), bf16),
+            pltpu.VMEM((4, hd, piece), bf16),
+            pltpu.VMEM((rows, 2 * ff), f32),
+            pltpu.VMEM((rows, ff), bf16),
+            pltpu.VMEM((rows, hd), bf16),
+            pltpu.VMEM((2, 4, own, width), bf16),
+            pltpu.VMEM((4, own, width), bf16),
+            pltpu.VMEM((3, own, width), bf16),
+            pltpu.VMEM((3, own, width), bf16),
+            dma((5, 16)), dma((5, 7)), dma((5, 8)),
+            dma((chunks, 8)), dma((chunks, 7)),
+            dma((chunks,)), dma((chunks,)), dma((chunks, 3)), dma((chunks, 3)),
+        ],
+        compiler_params=pltpu.CompilerParams(
+            collective_id=0, has_side_effects=True, vmem_limit_bytes=63 * 2**20
+        ),
+    )(*operands)
+
+
 def solution(mesh):
     n_fs, n_tp = mesh.shape["fs"], mesh.shape["tp"]
     share = math.gcd(math.gcd(HEADS // n_tp, n_fs), 4)
-    body = make_body(n_fs, n_tp, share)
+    if (n_fs, n_tp, share) == (16, 2, 4):
+        body = fused_body
+    else:
+        body = make_body(n_fs, n_tp, share)
     in_specs = (
         P(("fs", "tp"), None),
         P(),

time: 653 us -> 356 us (0.55)
  waiting for transfers between devices: 455 us -> 0 us
  Pallas kernels: 0 us -> 346 us
  blocking collectives: 56 us -> 0 us
  matrix products: 52.5 us -> 0 us
  local copies, waits for them, and re-layouts: 43.4 us -> 8.66 us
  other arithmetic: 30.5 us -> 1.33 us
  between operations: 13.7 us -> 0.01 us
    pallas_call x0 -> x1, Pallas kernels: none -> 346 us  [fused_body(): pl.pallas_call(fused_kernel, out_shape=jax.ShapeDtypeStruct((own, width),...]
    all_gather x6 -> x0, waiting for transfers between devices: 321 us -> none  [the longest x3 224 us: fetch(): lax.all_gather(swapped, 'fs', axis=0, axis_index_groups=twins, tiled=False)]
    reduce_scatter x3 -> x0, waiting for transfers between devices: 134 us -> none  [return_rows(): lax.psum_scatter(term.astype(jnp.bfloat16), ('fs', 'tp'), scatter_dimensi...]
    all_to_all x3 -> x0, blocking collectives: 56 us -> none  [fetch(): lax.all_to_all(pieces, 'fs', split_axis=0, concat_axis=0, axis_index_grou...]
    dot_general x9 -> x0, matrix products: 52.5 us -> none  [the longest x2 20.3 us: half_step(): both = jnp.dot(inputs, entry, preferred_element_type=jnp.float32)]
    convert_element_type x8 -> x0, other arithmetic: 10 us -> none  [the longest x3 4.01 us: normalize(): return (scaled * gain_vector).astype(jnp.bfloat16)]
    slice x4 -> x0, local copies, waits for them, and re-layouts: 9.99 us -> none  [the longest x1 4.1 us: body(): down_full = leave[:hidden_width]]
  transfers between devices with their start and end apart: 9 -> 0, of which waited for: 9 -> 0; matrix products, arithmetic and copies ran while one was open for 5% -> 0% of each run, Pallas kernels for 0% -> 0%
where the time goes in v1:
time: 356 us
  Pallas kernels  346 us (97%)
  local copies, waits for them, and re-layouts  8.66 us (2%)
    pallas_call x1, Pallas kernels, fused_body(): pl.pallas_call(fused_kernel, out_shape=jax.ShapeDtypeStruct((own, width),...  346 us

profile of v1, /device:TPU:0, one launch (start us, length us, event | category | flops | bytes accessed | tf_op | source)
XLA Modules:
  0.0 355.9 jit_solution(7605341941062272823)
XLA Ops:
  0.0 0.1 pad.2.clone
  0.1 1.3 dynamic_slice.17
  1.4 1.3 dynamic_slice.18
  2.7 1.3 dynamic_slice.19
  4.1 1.3 maximum_maximum_fusion.scales_ref
  5.4 0.8 dynamic_slice.15
  6.2 0.6 reshape.27.gs_ref
  6.8 0.8 dynamic_slice.16
  7.5 0.6 reshape.28.us_ref
  8.1 345.9 %shard_map.190 = bf16[128,2048]{1,0:T(8,128)(2,1)} custom-call(bf16[128,2048]{1,0:T(8,128)(2,1)} %res_ref.1, f32[1,2048]{1,0:T(1,128)} %bitcast.8, f32[1,2048]{1,0:T(1,128)} %bitcast.9, f32[1,2048]{1,0:T(1,128)} %bitcast.10, f32[128,3072]{1,0:T(8,128)} %gate_ref.1, f32[128,3072]{1,0:T(8,128)} %up_ref.1, f32[3072,128]{1,0:T(8,128)} %down_ref.1, ...), custom_call_target="tpu_custom_call" | custom-call | tf_op jit(solution)/shard_map/pallas_call | solution.py:602
  354.0 1.9 copy.22
  (1 shorter events, 0.0 us)

commit v2 on v1

--- a/solution.py
+++ b/solution.py
@@ -241,18 +241,16 @@
 
 MESH = pl.DeviceIdType.MESH
 GU, DN, QKV, OUT, SC = range(5)
-FAR_FIRST = ((1, 0, 0), (1, 1, 0), (1, 0, 1), (1, 1, 1), (0, 1, 0), (0, 1, 1), (0, 0, 1))
-TEAM = ((1, 1), (1, 0), (0, 1))
-LAG_REDUCE, LAG_FINISH, LAG_PASS = 1, 3, 5
+PLANE = ((0, 0, 1), (0, 1, 0), (0, 1, 1), (1, 0, 0), (1, 1, 0), (1, 0, 1), (1, 1, 1))
 
 
 def fused_kernel(
     res_ref, g1_ref, g2_ref, g3_ref,
     gate_ref, up_ref, down_ref, q_ref, k_ref, v_ref, o_ref,
-    gs_ref, us_ref, qs_ref, ks_ref, vs_ref, scales_ref, cos_ref, sin_ref,
+    gs_ref, us_ref, qs_ref, ks_ref, vs_ref, ds_ref, os_ref, cos_ref, sin_ref,
     out_ref,
     rows_raw, rows_normed, w_gu, w_d, w_qkv, w_o, w_sc,
-    st_gu, st_d, st_qkv, st_o, acc, hidden, mixed, part, part_twin, chip_part, far_part,
+    st_gu, st_d, st_qkv, st_o, scales_ref, acc, hidden, mixed, part, part_twin, chip_part, far_part,
     w_recv, w_send, w_fwd, ag_recv, ag_send, tw_recv, tw_send, rs_recv, rs_send,
 ):
     f32, bf16 = jnp.float32, jnp.bfloat16
@@ -280,7 +278,7 @@
         )
 
     barrier = pltpu.get_barrier_semaphore()
-    for dh, dl, dx in FAR_FIRST:
+    for dh, dl, dx in PLANE:
         peer, _ = plane_peer(dh, dl, dx)
         pl.semaphore_signal(barrier, inc=1, device_id=(peer, t), device_id_type=MESH)
     pl.semaphore_signal(barrier, inc=1, device_id=(f_y, t), device_id_type=MESH)
@@ -304,8 +302,9 @@
         return {GU: st_gu, DN: st_d, QKV: st_qkv, OUT: st_o}[kind].at[m]
 
     def send_pieces(kind):
-        remote(staged(kind, me), slot(kind, f), w_fwd.at[kind, me], w_recv.at[kind, f], f_y, t).start()
-        for i, (dh, dl, dx) in enumerate(FAR_FIRST):
+        own_place = me if kind == DN else x
+        remote(staged(kind, me), slot(kind, f), w_fwd.at[kind, own_place], w_recv.at[kind, f], f_y, t).start()
+        for i, (dh, dl, dx) in enumerate(PLANE):
             peer, m = plane_peer(dh, dl, dx)
             remote(staged(kind, m), slot(kind, f), w_send.at[kind, i], w_recv.at[kind, f], peer, t).start()
         slot(kind, f)[...] = staged(kind, me)[...]
@@ -314,8 +313,12 @@
         zz = 2 * ((zh + (j // 2) % 2) % 2) + j % 2
         return zz * 4 + ((y + j // 4) % 2) * 2
 
+    def near_base(j):
+        zz = 2 * ((zh + (j // 2) % 2) % 2) + (zl + j) % 2
+        return zz * 4 + ((y + j // 4) % 2) * 2
+
     def take_pair(kind, j):
-        base = pair_base(j)
+        base = pair_base(j) if kind == DN else near_base(j)
         for xx in (0, 1):
             s = base + xx
 
@@ -337,7 +340,7 @@
         lax.fori_loop(0, 8, step, 0)
 
     def finish_sends(kind):
-        for i, (dh, dl, dx) in enumerate(FAR_FIRST):
+        for i, (dh, dl, dx) in enumerate(PLANE):
             peer, m = plane_peer(dh, dl, dx)
             remote(staged(kind, m), slot(kind, f), w_send.at[kind, i], w_recv.at[kind, f], peer, t).wait_send()
         for i in range(8):
@@ -353,17 +356,29 @@
         dst = rows_raw.at[block_rows(m, core), pl.ds(column(j), chunk)]
         return remote(dst if src is None else src, dst, ag_send.at[j, i], ag_recv.at[j, m * 2 + core], fs, tp)
 
-    def ag_start(j, src):
-        for i, (dl, dx) in enumerate(TEAM):
-            peer, _ = plane_peer(0, dl, dx)
-            ag_copy(j, i, src, me, t, peer, t).start()
-        ag_copy(j, 3, src, me, t, f, 1 - t).start()
-
-    def ag_pass(j):
-        for i, (dl, dx) in enumerate(TEAM):
-            _, m = plane_peer(0, dl, dx)
-            ag_copy(j, 4 + i, None, m, t, f, 1 - t).wait_recv()
-            ag_copy(j, 4 + i, None, m, t, f, 1 - t).start()
+    def way(dl, dx):
+        first, m_first = plane_peer(0, dl, dx)
+        second, m_second = plane_peer(0, 1 - dl, 1 - dx)
+        return first, second, m_first, m_second, plane_peer(0, 1, 1)[1]
+
+    z_then_x, x_then_z, by_core = way(1, 0), way(0, 1), way(t, 1 - t)
+
+    def ag_start(j, src, route):
+        first, second, _, _, _ = route
+        ag_copy(j, 0, src, me, t, first, t).start()
+        ag_copy(j, 1, src, me, t, second, t).start()
+        ag_copy(j, 2, src, me, t, f, 1 - t).start()
+
+    def ag_relay(j, route):
+        _, second, m_first, _, _ = route
+        ag_copy(j, 3, None, m_first, t, second, t).wait_recv()
+        ag_copy(j, 3, None, m_first, t, second, t).start()
+        ag_copy(j, 4, None, m_first, t, f, 1 - t).start()
+
+    def ag_pass(j, route):
+        for i, m in enumerate(route[3:]):
+            ag_copy(j, 5 + i, None, m, t, f, 1 - t).wait_recv()
+            ag_copy(j, 5 + i, None, m, t, f, 1 - t).start()
 
     def ag_finish():
         def step(j, _):
@@ -392,10 +407,17 @@
 
         lax.fori_loop(0, rows_raw.shape[0] // size, step, 0)
 
-    def accumulate(kind, weights, columns):
+    def clear(columns):
+        def tile(r):
+            acc[r, :columns] = jnp.zeros((seq, columns), f32)
+
+        row_tiles(seq, tile)
+
+    def accumulate(kind, weights, columns, begin, end, take):
         def step(j, _):
-            take_pair(kind, j)
-            at = pl.ds(column(j), chunk)
+            if take:
+                take_pair(kind, j)
+            at = pl.ds(pl.multiple_of(near_base(j) * piece, chunk), chunk)
 
             def tile(r):
                 acc[r, :columns] += jnp.dot(rows_normed[r, at], weights[at, :], preferred_element_type=f32)
@@ -403,17 +425,13 @@
             row_tiles(seq, tile)
             return 0
 
-        def clear(r):
-            acc[r, :columns] = jnp.zeros((seq, columns), f32)
-
-        row_tiles(seq, clear)
-        lax.fori_loop(0, 8, step, 0)
+        lax.fori_loop(begin, end, step, 0)
 
     def silu_mul(gate, up):
-        gate = gate * gs_ref[...]
-        return (gate / (1.0 + jnp.exp(-gate)) * (up * us_ref[...])).astype(bf16)
-
-    def leave(inputs, weights, scale_row, factor, arriving, last):
+        gate = gate * gs_ref[:, pl.ds(pl.multiple_of(me * ff, ff), ff)]
+        return (gate / (1.0 + jnp.exp(-gate)) * (up * us_ref[:, pl.ds(pl.multiple_of(me * ff, ff), ff)])).astype(bf16)
+
+    def leave(inputs, weights, scale_row, factor, arriving, last, sums, rows, lags, during=None):
         def product(j):
             if arriving is not None:
                 take_pair(arriving, j)
@@ -438,63 +456,85 @@
             at = pl.ds(column(j), chunk)
             return remote(part.at[1 - t, :, :, at], part_twin.at[:, :, at], tw_send.at[j], tw_recv.at[j], f, 1 - t)
 
-        def to_team(j, i):
-            dl, dx = TEAM[i]
+        first, second, m_first, m_second, m_third = sums
+
+        def to_first(j):
             at = pl.ds(column(j), chunk)
-            peer, _ = plane_peer(0, dl, dx)
-            return remote(chip_part.at[i, :, at], far_part.at[i, :, at], rs_send.at[j, i], rs_recv.at[j, i], peer, t)
+            pair = pl.ds(0, 2)
+            return remote(
+                chip_part.at[pair, :, at], far_part.at[pair, :, at], rs_send.at[j, 0], rs_recv.at[j, 0], first, t
+            )
+
+        def to_second(j):
+            at = pl.ds(column(j), chunk)
+            return remote(chip_part.at[2, :, at], far_part.at[2, :, at], rs_send.at[j, 1], rs_recv.at[j, 1], second, t)
+
+        def chip_sum(m, at):
+            return part[t, m, :, at].astype(f32) + part_twin[m, :, at].astype(f32)
 
         def reduce(j):
             at = pl.ds(column(j), chunk)
             to_twin(j).wait_recv()
-            for i, (dl, dx) in enumerate(TEAM):
-                _, m = plane_peer(0, dl, dx)
-                chip_part[i, :, at] = (part[t, m, :, at].astype(f32) + part_twin[m, :, at].astype(f32)).astype(bf16)
-                to_team(j, i).start()
+            chip_part[0, :, at] = chip_sum(m_first, at).astype(bf16)
+            chip_part[1, :, at] = chip_sum(m_third, at).astype(bf16)
+            to_first(j).start()
+
+        def relay(j):
+            at = pl.ds(column(j), chunk)
+            to_first(j).wait_recv()
+            chip_part[2, :, at] = (chip_sum(m_second, at) + far_part[1, :, at].astype(f32)).astype(bf16)
+            to_second(j).start()
 
         def finish(j):
             at = pl.ds(column(j), chunk)
-            total = part[t, me, :, at].astype(f32) + part_twin[me, :, at].astype(f32)
-            for i in range(3):
-                to_team(j, i).wait_recv()
-                total = total + far_part[i, :, at].astype(f32)
+            to_second(j).wait_recv()
+            total = chip_sum(me, at) + far_part[0, :, at].astype(f32) + far_part[2, :, at].astype(f32)
             mine = block_rows(me, t)
             fresh = (rows_raw[mine, at].astype(f32) + factor * total).astype(bf16)
             if last:
                 out_ref[:, at] = fresh
             else:
                 rows_raw[mine, at] = fresh
-                ag_start(j, None)
+                ag_start(j, None, rows)
+
+        stages = [product, reduce, relay, finish]
+        if not last:
+            stages += [lambda j: ag_relay(j, rows), lambda j: ag_pass(j, rows)]
 
         def step(i, _):
-            pl.when(i < chunks)(lambda: product(i))
-            j_reduce, j_finish, j_pass = i - LAG_REDUCE, i - LAG_FINISH, i - LAG_PASS
-            pl.when((j_reduce >= 0) & (j_reduce < chunks))(lambda: reduce(j_reduce))
-            pl.when((j_finish >= 0) & (j_finish < chunks))(lambda: finish(j_finish))
-            if not last:
-                pl.when(j_pass >= 0)(lambda: ag_pass(j_pass))
+            for lag, stage in zip(lags, stages):
+                pl.when((i >= lag) & (i < chunks + lag))(lambda stage=stage, lag=lag: stage(i - lag))
+            if during is not None:
+                during(i)
             return 0
 
-        lax.fori_loop(0, chunks + (LAG_FINISH if last else LAG_PASS), step, 0)
+        lax.fori_loop(0, chunks + lags[len(stages) - 1], step, 0)
 
         def drain(j, _):
             to_twin(j).wait_send()
-            for i in range(3):
-                to_team(j, i).wait_send()
+            to_first(j).wait_send()
+            to_second(j).wait_send()
             return 0
 
         lax.fori_loop(0, chunks, drain, 0)
         if not last:
             ag_finish()
 
-    def first_rows(j, _):
-        ag_start(j, res_ref.at[:, pl.ds(column(j), chunk)])
-        return 0
-
-    lax.fori_loop(0, chunks, first_rows, 0)
+    def each_chunk(body):
+        def step(j, _):
+            body(j)
+            return 0
+
+        lax.fori_loop(0, chunks, step, 0)
+
+    scales_ref[...] = jnp.zeros_like(scales_ref)
+    scales_ref[0:1, :] = ds_ref[...]
+    scales_ref[1:2, :] = os_ref[...]
+    send_pieces(SC)
+
+    each_chunk(lambda j: ag_start(j, res_ref.at[:, pl.ds(column(j), chunk)], z_then_x))
     rows_raw[block_rows(me, t), :] = res_ref[...]
 
-    send_pieces(SC)
     for m in range(4):
         at = slice(m * ff, (m + 1) * ff)
         st_gu[m, :, :ff] = gate_ref[:, at].astype(bf16)
@@ -512,25 +552,32 @@
     send_pieces(QKV)
     send_pieces(OUT)
 
-    def first_pass(j, _):
-        ag_pass(j)
-        return 0
-
-    lax.fori_loop(0, chunks, first_pass, 0)
+    clear(2 * ff)
+    each_chunk(lambda j: ag_relay(j, z_then_x))
+    for j in range(3):
+        take_pair(GU, j)
+    each_chunk(lambda j: ag_pass(j, z_then_x))
     ag_finish()
     norm_rows(g1_ref)
+    take_pair(GU, 3)
+    accumulate(GU, w_gu, 2 * ff, 0, 4, False)
+    accumulate(GU, w_gu, 2 * ff, 4, 8, True)
     take_all(SC)
-
-    accumulate(GU, w_gu, 2 * ff)
 
     def first_hidden(r):
         hidden[r, :] = silu_mul(acc[r, :ff], acc[r, ff:])
 
     row_tiles(own, first_hidden)
-    leave(hidden, w_d, 0, 0.5, DN, False)
+
+    def take_qkv(i):
+        pl.when((i >= 7) & (i < 15) & (i % 2 == 1))(lambda: take_pair(QKV, (i - 7) // 2))
+
+    leave(hidden, w_d, 0, 0.5, DN, False, x_then_z, z_then_x, (0, 1, 4, 6, 7, 8), take_qkv)
 
     norm_rows(g2_ref)
-    accumulate(QKV, w_qkv, 3 * hd)
+    clear(3 * hd)
+    accumulate(QKV, w_qkv, 3 * hd, 0, 4, False)
+    accumulate(QKV, w_qkv, 3 * hd, 4, 8, True)
     take_all(OUT)
     head = (t * 4 + me).astype(f32)
     ri = lax.broadcasted_iota(jnp.int32, (seq, seq), 0)
@@ -539,22 +586,24 @@
     distance = jnp.maximum(ri - ci, 0).astype(f32)
     decay = jnp.where(ri >= ci, jnp.exp(-rate * distance), 0.0) * hd ** (-0.5)
 
+    at_head = pl.ds(pl.multiple_of(me * hd, hd), hd)
+
     def turn(values):
         a, b = values[:, : hd // 2], values[:, hd // 2 :]
         c, s = cos_ref[...], sin_ref[...]
         return jnp.concatenate([a * c - b * s, b * c + a * s], axis=1).astype(bf16)
 
     def sequence(r):
-        q = turn(acc[r, :hd] * qs_ref[...])
-        k = turn(acc[r, hd : 2 * hd] * ks_ref[...])
-        v = (acc[r, 2 * hd : 3 * hd] * vs_ref[...]).astype(bf16)
+        q = turn(acc[r, :hd] * qs_ref[:, at_head])
+        k = turn(acc[r, hd : 2 * hd] * ks_ref[:, at_head])
+        v = (acc[r, 2 * hd : 3 * hd] * vs_ref[:, at_head]).astype(bf16)
         scores = lax.dot_general(q, k, (((1,), (1,)), ((), ())), preferred_element_type=f32)
         both = jnp.dot((scores * decay).astype(bf16), v, preferred_element_type=f32)
         level = jnp.maximum(jnp.mean(both * both, axis=-1, keepdims=True), HEAD_FLOOR)
         mixed[r, :] = (both * lax.rsqrt(level)).astype(bf16)
 
     row_tiles(seq, sequence)
-    leave(mixed, w_o, 1, 1.0, None, False)
+    leave(mixed, w_o, 1, 1.0, None, False, by_core, by_core, (0, 1, 3, 5, 7, 9))
 
     norm_rows(g3_ref)
 
@@ -564,7 +613,7 @@
         hidden[r, :] = silu_mul(gate, up)
 
     row_tiles(seq, second_hidden)
-    leave(hidden, w_d, 0, 0.5, None, True)
+    leave(hidden, w_d, 0, 0.5, None, True, by_core, by_core, (0, 1, 3, 5))
     for kind in (SC, GU, DN, QKV, OUT):
         finish_sends(kind)
 
@@ -580,23 +629,19 @@
     rows, piece = 8 * own, gate_weight.shape[0]
     ff, hd = gate_weight.shape[1] // 4, query_weight.shape[1] // 4
     chunks = width // (2 * piece)
-    x, z = lax.axis_index("fs") % 2, lax.axis_index("fs") // 4
-    me = (z % 2) * 2 + x
-
-    def part_of(vector, size):
-        return lax.dynamic_slice_in_dim(vector, me * size, size).reshape(1, -1)
-
-    scales = jnp.concatenate([down_scale[None], output_scale[None], jnp.zeros((6, piece), f32)])
+
+    def row(vector):
+        return vector.reshape(1, -1)
+
     half = hd // 2
     frequency = np.float32(ROTARY_BASE) ** (-np.arange(half, dtype=np.float32) * np.float32(2.0) / np.float32(hd))
     angles = np.arange(2 * own, dtype=np.float32)[:, None] * frequency.astype(np.float32)[None]
     cosine, sine_value = np.cos(angles).astype(np.float32), np.sin(angles).astype(np.float32)
     operands = (
-        residual_in, gain_first.reshape(1, -1), gain_mixer.reshape(1, -1), gain_second.reshape(1, -1),
+        residual_in, row(gain_first), row(gain_mixer), row(gain_second),
         gate_weight, up_weight, down_weight, query_weight, key_weight, value_weight, output_weight,
-        part_of(gate_scale, ff), part_of(up_scale, ff),
-        part_of(query_scale, hd), part_of(key_scale, hd), part_of(value_scale, hd),
-        scales, jnp.asarray(cosine), jnp.asarray(sine_value),
+        row(gate_scale), row(up_scale), row(query_scale), row(key_scale), row(value_scale),
+        row(down_scale), row(output_scale), jnp.asarray(cosine), jnp.asarray(sine_value),
     )
     dma = pltpu.SemaphoreType.DMA
     return pl.pallas_call(
@@ -616,6 +661,7 @@
             pltpu.VMEM((4, ff, piece), bf16),
             pltpu.VMEM((4, piece, 3 * hd), bf16),
             pltpu.VMEM((4, hd, piece), bf16),
+            pltpu.VMEM((8, piece), f32),
             pltpu.VMEM((rows, 2 * ff), f32),
             pltpu.VMEM((rows, ff), bf16),
             pltpu.VMEM((rows, hd), bf16),
@@ -625,7 +671,7 @@
             pltpu.VMEM((3, own, width), bf16),
             dma((5, 16)), dma((5, 7)), dma((5, 8)),
             dma((chunks, 8)), dma((chunks, 7)),
-            dma((chunks,)), dma((chunks,)), dma((chunks, 3)), dma((chunks, 3)),
+            dma((chunks,)), dma((chunks,)), dma((chunks, 2)), dma((chunks, 2)),
         ],
         compiler_params=pltpu.CompilerParams(
             collective_id=0, has_side_effects=True, vmem_limit_bytes=63 * 2**20

time: 356 us -> 296 us (0.83)
  Pallas kernels: 346 us -> 294 us
  local copies, waits for them, and re-layouts: 8.66 us -> 1.88 us
    pallas_call x1, Pallas kernels: 346 us -> 294 us  [fused_body(): pl.pallas_call(fused_kernel, out_shape=jax.ShapeDtypeStruct((own, width),...]
    dynamic_slice x5 -> x0, local copies, waits for them, and re-layouts: 5.51 us -> none  [part_of(): return lax.dynamic_slice_in_dim(vector, me * size, size).reshape(1, -1)]
where the time goes in v2:
time: 296 us
  Pallas kernels  294 us (99%)
    pallas_call x1, Pallas kernels, fused_body(): pl.pallas_call(fused_kernel, out_shape=jax.ShapeDtypeStruct((own, width),...  294 us

profile of v2, /device:TPU:0, one launch (start us, length us, event | category | flops | bytes accessed | tf_op | source)
XLA Modules:
  0.0 296.3 jit_solution(9086181129032176951)
XLA Ops:
  0.0 294.4 %shard_map.190 = bf16[128,2048]{1,0:T(8,128)(2,1)} custom-call(bf16[128,2048]{1,0:T(8,128)(2,1)} %res_ref.1, f32[1,2048]{1,0:T(1,128)} %bitcast.12, f32[1,2048]{1,0:T(1,128)} %bitcast.13, f32[1,2048]{1,0:T(1,128)} %bitcast.14, f32[128,3072]{1,0:T(8,128)} %gate_ref.1, f32[128,3072]{1,0:T(8,128)} %up_ref.1, f32[3072,128]{1,0:T(8,128)} %down_ref.1, ...), custom_call_target="tpu_custom_call" | custom-call | tf_op jit(solution)/shard_map/pallas_call | solution.py:647
  294.4 1.9 copy.22

commit v3 on v2

--- a/solution.py
+++ b/solution.py
@@ -240,7 +240,7 @@
 
 
 MESH = pl.DeviceIdType.MESH
-GU, DN, QKV, OUT, SC = range(5)
+GATE, UP, DN, QKV, OUT, SC = range(6)
 PLANE = ((0, 0, 1), (0, 1, 0), (0, 1, 1), (1, 0, 0), (1, 1, 0), (1, 0, 1), (1, 1, 1))
 
 
@@ -286,8 +286,8 @@
     pl.semaphore_wait(barrier, 9)
 
     def slot(kind, s):
-        if kind == GU:
-            return w_gu.at[pl.ds(pl.multiple_of(s * piece, piece), piece), :]
+        if kind in (GATE, UP):
+            return w_gu.at[pl.ds(pl.multiple_of(s * piece, piece), piece), pl.ds(kind * ff, ff)]
         if kind == DN:
             return w_d.at[:, pl.ds(pl.multiple_of(s * piece, piece), piece)]
         if kind == QKV:
@@ -299,15 +299,27 @@
     def staged(kind, m):
         if kind == SC:
             return scales_ref
-        return {GU: st_gu, DN: st_d, QKV: st_qkv, OUT: st_o}[kind].at[m]
-
-    def send_pieces(kind):
+        if kind in (GATE, UP):
+            return st_gu.at[m, :, pl.ds(kind * ff, ff)]
+        return {DN: st_d, QKV: st_qkv, OUT: st_o}[kind].at[m]
+
+    def send_near(kind):
         own_place = me if kind == DN else x
         remote(staged(kind, me), slot(kind, f), w_fwd.at[kind, own_place], w_recv.at[kind, f], f_y, t).start()
-        for i, (dh, dl, dx) in enumerate(PLANE):
-            peer, m = plane_peer(dh, dl, dx)
+        send_some(kind, 0, 3)
+        slot(kind, f)[...] = staged(kind, me)[...]
+
+    def send_far(kind):
+        send_some(kind, 3, 7)
+
+    def send_some(kind, begin, end):
+        for i in range(begin, end):
+            peer, m = plane_peer(*PLANE[i])
             remote(staged(kind, m), slot(kind, f), w_send.at[kind, i], w_recv.at[kind, f], peer, t).start()
-        slot(kind, f)[...] = staged(kind, me)[...]
+
+    def send_pieces(kind):
+        send_near(kind)
+        send_far(kind)
 
     def pair_base(j):
         zz = 2 * ((zh + (j // 2) % 2) % 2) + j % 2
@@ -332,12 +344,12 @@
                     slot(kind, s), slot(kind, s), w_fwd.at[kind, (j % 4) * 2 + xx], w_recv.at[kind, s], f_y, t
                 ).start()
 
-    def take_all(kind):
+    def take_some(kind, begin, end):
         def step(j, _):
             take_pair(kind, j)
             return 0
 
-        lax.fori_loop(0, 8, step, 0)
+        lax.fori_loop(begin, end, step, 0)
 
     def finish_sends(kind):
         for i, (dh, dl, dx) in enumerate(PLANE):
@@ -406,26 +418,6 @@
             return 0
 
         lax.fori_loop(0, rows_raw.shape[0] // size, step, 0)
-
-    def clear(columns):
-        def tile(r):
-            acc[r, :columns] = jnp.zeros((seq, columns), f32)
-
-        row_tiles(seq, tile)
-
-    def accumulate(kind, weights, columns, begin, end, take):
-        def step(j, _):
-            if take:
-                take_pair(kind, j)
-            at = pl.ds(pl.multiple_of(near_base(j) * piece, chunk), chunk)
-
-            def tile(r):
-                acc[r, :columns] += jnp.dot(rows_normed[r, at], weights[at, :], preferred_element_type=f32)
-
-            row_tiles(seq, tile)
-            return 0
-
-        lax.fori_loop(begin, end, step, 0)
 
     def silu_mul(gate, up):
         gate = gate * gs_ref[:, pl.ds(pl.multiple_of(me * ff, ff), ff)]
@@ -532,53 +524,72 @@
     scales_ref[1:2, :] = os_ref[...]
     send_pieces(SC)
 
-    each_chunk(lambda j: ag_start(j, res_ref.at[:, pl.ds(column(j), chunk)], z_then_x))
-    rows_raw[block_rows(me, t), :] = res_ref[...]
-
     for m in range(4):
         at = slice(m * ff, (m + 1) * ff)
         st_gu[m, :, :ff] = gate_ref[:, at].astype(bf16)
-        st_gu[m, :, ff:] = up_ref[:, at].astype(bf16)
-    send_pieces(GU)
+    send_pieces(GATE)
+    each_chunk(lambda j: ag_start(j, res_ref.at[:, pl.ds(column(j), chunk)], z_then_x))
+    rows_raw[block_rows(me, t), :] = res_ref[...]
+
     for m in range(4):
-        st_d[m] = down_ref[m * ff : (m + 1) * ff, :].astype(bf16)
-    send_pieces(DN)
+        st_gu[m, :, ff:] = up_ref[:, m * ff : (m + 1) * ff].astype(bf16)
+    send_pieces(UP)
     for m in range(4):
         at = slice(m * hd, (m + 1) * hd)
+        st_d[m] = down_ref[m * ff : (m + 1) * ff, :].astype(bf16)
         st_qkv[m, :, :hd] = q_ref[:, at].astype(bf16)
         st_qkv[m, :, hd : 2 * hd] = k_ref[:, at].astype(bf16)
         st_qkv[m, :, 2 * hd :] = v_ref[:, at].astype(bf16)
         st_o[m] = o_ref[at, :].astype(bf16)
-    send_pieces(QKV)
-    send_pieces(OUT)
-
-    clear(2 * ff)
+
+    ahead = zl != zh
+    take_some(SC, 0, 4)
+    take_some(GATE, 0, 4)
     each_chunk(lambda j: ag_relay(j, z_then_x))
-    for j in range(3):
-        take_pair(GU, j)
+    pl.when(ahead)(lambda: send_pieces(DN))
+    pl.when(jnp.logical_not(ahead))(lambda: send_near(DN))
+    send_near(QKV)
+    send_near(OUT)
+    take_some(UP, 0, 2)
     each_chunk(lambda j: ag_pass(j, z_then_x))
     ag_finish()
     norm_rows(g1_ref)
-    take_pair(GU, 3)
-    accumulate(GU, w_gu, 2 * ff, 0, 4, False)
-    accumulate(GU, w_gu, 2 * ff, 4, 8, True)
-    take_all(SC)
+    take_some(UP, 2, 3)
+    take_some(GATE, 4, 8)
+
+    def first_gate(r):
+        acc[r, :ff] = jnp.dot(rows_normed[r, :], w_gu[:, :ff], preferred_element_type=f32)
+
+    row_tiles(seq, first_gate)
+    take_some(UP, 3, 4)
+    pl.when(ahead)(lambda: send_far(QKV))
+    pl.when(jnp.logical_not(ahead))(lambda: send_far(DN))
+    take_some(UP, 4, 8)
+    take_some(SC, 4, 8)
 
     def first_hidden(r):
-        hidden[r, :] = silu_mul(acc[r, :ff], acc[r, ff:])
-
-    row_tiles(own, first_hidden)
-
-    def take_qkv(i):
+        up = jnp.dot(rows_normed[r, :], w_gu[:, ff:], preferred_element_type=f32)
+        hidden[r, :] = silu_mul(acc[r, :ff], up)
+
+    row_tiles(seq, first_hidden)
+
+    def take_early(i):
+        pl.when((i == 3) & ahead)(lambda: send_far(OUT))
+        pl.when((i == 3) & jnp.logical_not(ahead))(lambda: send_far(QKV))
+        pl.when((i == 8) & jnp.logical_not(ahead))(lambda: send_far(OUT))
         pl.when((i >= 7) & (i < 15) & (i % 2 == 1))(lambda: take_pair(QKV, (i - 7) // 2))
-
-    leave(hidden, w_d, 0, 0.5, DN, False, x_then_z, z_then_x, (0, 1, 4, 6, 7, 8), take_qkv)
+        pl.when(i >= 14)(lambda: take_pair(OUT, i - 14))
+
+    leave(hidden, w_d, 0, 0.5, DN, False, x_then_z, by_core, (0, 1, 4, 6, 8, 10), take_early)
 
     norm_rows(g2_ref)
-    clear(3 * hd)
-    accumulate(QKV, w_qkv, 3 * hd, 0, 4, False)
-    accumulate(QKV, w_qkv, 3 * hd, 4, 8, True)
-    take_all(OUT)
+    take_some(QKV, 4, 8)
+
+    def project(r):
+        acc[r, : 3 * hd] = jnp.dot(rows_normed[r, :], w_qkv[...], preferred_element_type=f32)
+
+    row_tiles(seq, project)
+    take_some(OUT, 4, 8)
     head = (t * 4 + me).astype(f32)
     ri = lax.broadcasted_iota(jnp.int32, (seq, seq), 0)
     ci = lax.broadcasted_iota(jnp.int32, (seq, seq), 1)
@@ -614,7 +625,7 @@
 
     row_tiles(seq, second_hidden)
     leave(hidden, w_d, 0, 0.5, None, True, by_core, by_core, (0, 1, 3, 5))
-    for kind in (SC, GU, DN, QKV, OUT):
+    for kind in (SC, GATE, UP, DN, QKV, OUT):
         finish_sends(kind)
 
 
@@ -662,14 +673,14 @@
             pltpu.VMEM((4, piece, 3 * hd), bf16),
             pltpu.VMEM((4, hd, piece), bf16),
             pltpu.VMEM((8, piece), f32),
-            pltpu.VMEM((rows, 2 * ff), f32),
+            pltpu.VMEM((rows, max(ff, 3 * hd)), f32),
             pltpu.VMEM((rows, ff), bf16),
             pltpu.VMEM((rows, hd), bf16),
             pltpu.VMEM((2, 4, own, width), bf16),
             pltpu.VMEM((4, own, width), bf16),
             pltpu.VMEM((3, own, width), bf16),
             pltpu.VMEM((3, own, width), bf16),
-            dma((5, 16)), dma((5, 7)), dma((5, 8)),
+            dma((6, 16)), dma((6, 7)), dma((6, 8)),
             dma((chunks, 8)), dma((chunks, 7)),
             dma((chunks,)), dma((chunks,)), dma((chunks, 2)), dma((chunks, 2)),
         ],

time: 296 us -> 267 us (0.902)
  Pallas kernels: 294 us -> 265 us
    pallas_call x1, Pallas kernels: 294 us -> 265 us  [fused_body(): pl.pallas_call(fused_kernel, out_shape=jax.ShapeDtypeStruct((own, width),...]
where the time goes in v3:
time: 267 us
  Pallas kernels  265 us (99%)
    pallas_call x1, Pallas kernels, fused_body(): pl.pallas_call(fused_kernel, out_shape=jax.ShapeDtypeStruct((own, width),...  265 us

profile of v3, /device:TPU:0, one launch (start us, length us, event | category | flops | bytes accessed | tf_op | source)
XLA Modules:
  0.0 267.3 jit_solution(11848843867064790722)
XLA Ops:
  0.0 265.4 %shard_map.190 = bf16[128,2048]{1,0:T(8,128)(2,1)} custom-call(bf16[128,2048]{1,0:T(8,128)(2,1)} %res_ref.1, f32[1,2048]{1,0:T(1,128)} %bitcast.12, f32[1,2048]{1,0:T(1,128)} %bitcast.13, f32[1,2048]{1,0:T(1,128)} %bitcast.14, f32[128,3072]{1,0:T(8,128)} %gate_ref.1, f32[128,3072]{1,0:T(8,128)} %up_ref.1, f32[3072,128]{1,0:T(8,128)} %down_ref.1, ...), custom_call_target="tpu_custom_call" | custom-call | tf_op jit(solution)/shard_map/pallas_call | solution.py:658
  265.4 1.9 copy.22

commit v4 on v3

--- a/solution.py
+++ b/solution.py
@@ -244,13 +244,20 @@
 PLANE = ((0, 0, 1), (0, 1, 0), (0, 1, 1), (1, 0, 0), (1, 1, 0), (1, 0, 1), (1, 1, 1))
 
 
+EARLY = (
+    (4, QKV, 0), (5, QKV, 1), (9, QKV, 2), (11, QKV, 3), (12, OUT, 0), (12, OUT, 1), (13, OUT, 2), (13, OUT, 3),
+    (15, QKV, 4), (15, QKV, 5), (17, QKV, 6), (17, QKV, 7)
+)
+
+
 def fused_kernel(
     res_ref, g1_ref, g2_ref, g3_ref,
-    gate_ref, up_ref, down_ref, q_ref, k_ref, v_ref, o_ref,
+    gate_hbm, up_hbm, down_hbm, q_hbm, k_hbm, v_hbm, o_hbm,
     gs_ref, us_ref, qs_ref, ks_ref, vs_ref, ds_ref, os_ref, cos_ref, sin_ref,
     out_ref,
     rows_raw, rows_normed, w_gu, w_d, w_qkv, w_o, w_sc,
-    st_gu, st_d, st_qkv, st_o, scales_ref, acc, hidden, mixed, part, part_twin, chip_part, far_part,
+    st_gu, st_d, st_qkv, st_o, scales_ref, acc, power, hidden, mixed, part, part_twin, chip_part, far_part,
+    gate_ref, up_ref, down_ref, q_ref, k_ref, v_ref, o_ref, in_sems,
     w_recv, w_send, w_fwd, ag_recv, ag_send, tw_recv, tw_send, rs_recv, rs_send,
 ):
     f32, bf16 = jnp.float32, jnp.bfloat16
@@ -277,6 +284,12 @@
             src_ref=src, dst_ref=dst, send_sem=send, recv_sem=recv, device_id=(fs, tp), device_id_type=MESH
         )
 
+    sources = (gate_hbm, up_hbm, down_hbm, q_hbm, k_hbm, v_hbm, o_hbm)
+    landed = (gate_ref, up_ref, down_ref, q_ref, k_ref, v_ref, o_ref)
+    loads = [pltpu.make_async_copy(a, b, in_sems.at[i]) for i, (a, b) in enumerate(zip(sources, landed))]
+    for load in loads:
+        load.start()
+
     barrier = pltpu.get_barrier_semaphore()
     for dh, dl, dx in PLANE:
         peer, _ = plane_peer(dh, dl, dx)
@@ -303,9 +316,11 @@
             return st_gu.at[m, :, pl.ds(kind * ff, ff)]
         return {DN: st_d, QKV: st_qkv, OUT: st_o}[kind].at[m]
 
-    def send_near(kind):
+    def send_across(kind):
         own_place = me if kind == DN else x
         remote(staged(kind, me), slot(kind, f), w_fwd.at[kind, own_place], w_recv.at[kind, f], f_y, t).start()
+
+    def send_near(kind):
         send_some(kind, 0, 3)
         slot(kind, f)[...] = staged(kind, me)[...]
 
@@ -318,6 +333,7 @@
             remote(staged(kind, m), slot(kind, f), w_send.at[kind, i], w_recv.at[kind, f], peer, t).start()
 
     def send_pieces(kind):
+        send_across(kind)
         send_near(kind)
         send_far(kind)
 
@@ -392,12 +408,17 @@
             ag_copy(j, 5 + i, None, m, t, f, 1 - t).wait_recv()
             ag_copy(j, 5 + i, None, m, t, f, 1 - t).start()
 
-    def ag_finish():
+    def ag_arrive(j):
+        for m in range(4):
+            ag_copy(j, 0, None, m, 1 - t, f, 1 - t).wait_recv()
+
+    def ag_settle(j):
+        for i in range(7):
+            ag_copy(j, i, None, me, t, f, 1 - t).wait_send()
+
+    def each_chunk(body):
         def step(j, _):
-            for m in range(4):
-                ag_copy(j, 0, None, m, 1 - t, f, 1 - t).wait_recv()
-            for i in range(7):
-                ag_copy(j, i, None, me, t, f, 1 - t).wait_send()
+            body(j)
             return 0
 
         lax.fori_loop(0, chunks, step, 0)
@@ -419,11 +440,41 @@
 
         lax.fori_loop(0, rows_raw.shape[0] // size, step, 0)
 
+    def absorber(gain_ref, weights):
+        columns = weights.shape[1]
+
+        def stage(j):
+            at = pl.ds(column(j), chunk)
+
+            @pl.when(j == 0)
+            def _():
+                def clear(r):
+                    acc[r, :columns] = jnp.zeros((seq, columns), f32)
+                    power[r, :] = jnp.zeros((seq, piece), f32)
+
+                row_tiles(seq, clear)
+
+            ag_arrive(j)
+
+            def tile(r):
+                v = rows_raw[r, at].astype(f32)
+                square = v * v
+                power[r, :] += square[:, :piece] + square[:, piece:]
+                v = (v * gain_ref[:, at]).astype(bf16)
+                acc[r, :columns] += jnp.dot(v, weights[at, :], preferred_element_type=f32)
+
+            row_tiles(seq, tile)
+
+        return stage
+
+    def row_factor(r):
+        return lax.rsqrt(jnp.sum(power[r, :], axis=-1, keepdims=True) / width + EPSILON)
+
     def silu_mul(gate, up):
         gate = gate * gs_ref[:, pl.ds(pl.multiple_of(me * ff, ff), ff)]
         return (gate / (1.0 + jnp.exp(-gate)) * (up * us_ref[:, pl.ds(pl.multiple_of(me * ff, ff), ff)])).astype(bf16)
 
-    def leave(inputs, weights, scale_row, factor, arriving, last, sums, rows, lags, during=None):
+    def leave(inputs, weights, scale_row, factor, arriving, last, sums, rows, lags, absorb=None, during=None):
         def product(j):
             if arriving is not None:
                 take_pair(arriving, j)
@@ -433,15 +484,16 @@
                 [w_sc[pl.ds((base + h) * 8 + scale_row, 1), :] for h in (0, 1)], axis=1
             )
 
-            def step(m, _):
-                r = pl.ds(pl.multiple_of(m * seq, seq), seq)
+            def step(i, _):
+                r = pl.ds(pl.multiple_of(i * 2 * seq, 2 * seq), 2 * seq)
                 term = jnp.dot(inputs[r, :], weights[:, at], preferred_element_type=f32) * factors
                 term = term.astype(bf16)
-                part[0, m, :, at] = term[:own]
-                part[1, m, :, at] = term[own:]
+                for m in range(2):
+                    for core in range(2):
+                        part[core, i * 2 + m, :, at] = term[(m * 2 + core) * own : (m * 2 + core + 1) * own]
                 return 0
 
-            lax.fori_loop(0, 4, step, 0)
+            lax.fori_loop(0, 2, step, 0)
             to_twin(j).start()
 
         def to_twin(j):
@@ -491,7 +543,7 @@
 
         stages = [product, reduce, relay, finish]
         if not last:
-            stages += [lambda j: ag_relay(j, rows), lambda j: ag_pass(j, rows)]
+            stages += [lambda j: ag_relay(j, rows), lambda j: ag_pass(j, rows), absorb]
 
         def step(i, _):
             for lag, stage in zip(lags, stages):
@@ -510,20 +562,14 @@
 
         lax.fori_loop(0, chunks, drain, 0)
         if not last:
-            ag_finish()
-
-    def each_chunk(body):
-        def step(j, _):
-            body(j)
-            return 0
-
-        lax.fori_loop(0, chunks, step, 0)
+            each_chunk(ag_settle)
 
     scales_ref[...] = jnp.zeros_like(scales_ref)
     scales_ref[0:1, :] = ds_ref[...]
     scales_ref[1:2, :] = os_ref[...]
     send_pieces(SC)
 
+    loads[0].wait()
     for m in range(4):
         at = slice(m * ff, (m + 1) * ff)
         st_gu[m, :, :ff] = gate_ref[:, at].astype(bf16)
@@ -531,9 +577,12 @@
     each_chunk(lambda j: ag_start(j, res_ref.at[:, pl.ds(column(j), chunk)], z_then_x))
     rows_raw[block_rows(me, t), :] = res_ref[...]
 
+    loads[1].wait()
     for m in range(4):
         st_gu[m, :, ff:] = up_ref[:, m * ff : (m + 1) * ff].astype(bf16)
     send_pieces(UP)
+    for load in loads[2:]:
+        load.wait()
     for m in range(4):
         at = slice(m * hd, (m + 1) * hd)
         st_d[m] = down_ref[m * ff : (m + 1) * ff, :].astype(bf16)
@@ -542,17 +591,21 @@
         st_qkv[m, :, 2 * hd :] = v_ref[:, at].astype(bf16)
         st_o[m] = o_ref[at, :].astype(bf16)
 
+    for kind in (DN, QKV, OUT):
+        send_across(kind)
+
     ahead = zl != zh
     take_some(SC, 0, 4)
     take_some(GATE, 0, 4)
     each_chunk(lambda j: ag_relay(j, z_then_x))
-    pl.when(ahead)(lambda: send_pieces(DN))
-    pl.when(jnp.logical_not(ahead))(lambda: send_near(DN))
+    send_near(DN)
+    pl.when(ahead)(lambda: send_far(DN))
     send_near(QKV)
     send_near(OUT)
     take_some(UP, 0, 2)
     each_chunk(lambda j: ag_pass(j, z_then_x))
-    ag_finish()
+    each_chunk(ag_arrive)
+    each_chunk(ag_settle)
     norm_rows(g1_ref)
     take_some(UP, 2, 3)
     take_some(GATE, 4, 8)
@@ -577,18 +630,11 @@
         pl.when((i == 3) & ahead)(lambda: send_far(OUT))
         pl.when((i == 3) & jnp.logical_not(ahead))(lambda: send_far(QKV))
         pl.when((i == 8) & jnp.logical_not(ahead))(lambda: send_far(OUT))
-        pl.when((i >= 7) & (i < 15) & (i % 2 == 1))(lambda: take_pair(QKV, (i - 7) // 2))
-        pl.when(i >= 14)(lambda: take_pair(OUT, i - 14))
-
-    leave(hidden, w_d, 0, 0.5, DN, False, x_then_z, by_core, (0, 1, 4, 6, 8, 10), take_early)
-
-    norm_rows(g2_ref)
-    take_some(QKV, 4, 8)
-
-    def project(r):
-        acc[r, : 3 * hd] = jnp.dot(rows_normed[r, :], w_qkv[...], preferred_element_type=f32)
-
-    row_tiles(seq, project)
+        for at, kind, j in EARLY:
+            pl.when(i == at)(lambda kind=kind, j=j: take_pair(kind, j))
+
+    leave(hidden, w_d, 0, 0.5, DN, False, x_then_z, by_core, (0, 1, 4, 7, 9, 11, 12), absorber(g2_ref, w_qkv), take_early)
+
     take_some(OUT, 4, 8)
     head = (t * 4 + me).astype(f32)
     ri = lax.broadcasted_iota(jnp.int32, (seq, seq), 0)
@@ -605,26 +651,24 @@
         return jnp.concatenate([a * c - b * s, b * c + a * s], axis=1).astype(bf16)
 
     def sequence(r):
-        q = turn(acc[r, :hd] * qs_ref[:, at_head])
-        k = turn(acc[r, hd : 2 * hd] * ks_ref[:, at_head])
-        v = (acc[r, 2 * hd : 3 * hd] * vs_ref[:, at_head]).astype(bf16)
+        factor = row_factor(r)
+        q = turn(acc[r, :hd] * factor * qs_ref[:, at_head])
+        k = turn(acc[r, hd : 2 * hd] * factor * ks_ref[:, at_head])
+        v = (acc[r, 2 * hd : 3 * hd] * factor * vs_ref[:, at_head]).astype(bf16)
         scores = lax.dot_general(q, k, (((1,), (1,)), ((), ())), preferred_element_type=f32)
         both = jnp.dot((scores * decay).astype(bf16), v, preferred_element_type=f32)
         level = jnp.maximum(jnp.mean(both * both, axis=-1, keepdims=True), HEAD_FLOOR)
         mixed[r, :] = (both * lax.rsqrt(level)).astype(bf16)
 
     row_tiles(seq, sequence)
-    leave(mixed, w_o, 1, 1.0, None, False, by_core, by_core, (0, 1, 3, 5, 7, 9))
-
-    norm_rows(g3_ref)
+    leave(mixed, w_o, 1, 1.0, None, False, by_core, by_core, (0, 1, 3, 6, 9, 12, 13), absorber(g3_ref, w_gu))
 
     def second_hidden(r):
-        gate = jnp.dot(rows_normed[r, :], w_gu[:, :ff], preferred_element_type=f32)
-        up = jnp.dot(rows_normed[r, :], w_gu[:, ff:], preferred_element_type=f32)
-        hidden[r, :] = silu_mul(gate, up)
-
-    row_tiles(seq, second_hidden)
-    leave(hidden, w_d, 0, 0.5, None, True, by_core, by_core, (0, 1, 3, 5))
+        factor = row_factor(r)
+        hidden[r, :] = silu_mul(acc[r, :ff] * factor, acc[r, ff : 2 * ff] * factor)
+
+    row_tiles(own, second_hidden)
+    leave(hidden, w_d, 0, 0.5, None, True, by_core, by_core, (0, 1, 4, 8))
     for kind in (SC, GATE, UP, DN, QKV, OUT):
         finish_sends(kind)
 
@@ -658,7 +702,7 @@
     return pl.pallas_call(
         fused_kernel,
         out_shape=jax.ShapeDtypeStruct((own, width), bf16),
-        in_specs=[pl.BlockSpec(memory_space=pltpu.VMEM)] * len(operands),
+        in_specs=[pl.BlockSpec(memory_space=pl.ANY if 4 <= i < 11 else pltpu.VMEM) for i in range(len(operands))],
         out_specs=pl.BlockSpec(memory_space=pltpu.VMEM),
         scratch_shapes=[
             pltpu.VMEM((rows, width), bf16),
@@ -673,13 +717,16 @@
             pltpu.VMEM((4, piece, 3 * hd), bf16),
             pltpu.VMEM((4, hd, piece), bf16),
             pltpu.VMEM((8, piece), f32),
-            pltpu.VMEM((rows, max(ff, 3 * hd)), f32),
+            pltpu.VMEM((rows, max(2 * ff, 3 * hd)), f32),
+            pltpu.VMEM((rows, piece), f32),
             pltpu.VMEM((rows, ff), bf16),
             pltpu.VMEM((rows, hd), bf16),
             pltpu.VMEM((2, 4, own, width), bf16),
             pltpu.VMEM((4, own, width), bf16),
             pltpu.VMEM((3, own, width), bf16),
             pltpu.VMEM((3, own, width), bf16),
+            *[pltpu.VMEM(operand.shape, f32) for operand in operands[4:11]],
+            dma((7,)),
             dma((6, 16)), dma((6, 7)), dma((6, 8)),
             dma((chunks, 8)), dma((chunks, 7)),
             dma((chunks,)), dma((chunks,)), dma((chunks, 2)), dma((chunks, 2)),

time: 267 us -> 251 us (0.940)
  Pallas kernels: 265 us -> 249 us
    pallas_call x1, Pallas kernels: 265 us -> 249 us  [fused_body(): pl.pallas_call(fused_kernel, out_shape=jax.ShapeDtypeStruct((own, width),...]
where the time goes in v4:
time: 251 us
  Pallas kernels  249 us (99%)
    pallas_call x1, Pallas kernels, fused_body(): pl.pallas_call(fused_kernel, out_shape=jax.ShapeDtypeStruct((own, width),...  249 us

profile of v4, /device:TPU:0, one launch (start us, length us, event | category | flops | bytes accessed | tf_op | source)
XLA Modules:
  0.0 250.7 jit_solution(15086901556456711866)
XLA Ops:
  0.0 248.8 %shard_map.190 = bf16[128,2048]{1,0:T(8,128)(2,1)} custom-call(bf16[128,2048]{1,0:T(8,128)(2,1)} %res_ref.1, f32[1,2048]{1,0:T(1,128)} %bitcast.12, f32[1,2048]{1,0:T(1,128)} %bitcast.13, f32[1,2048]{1,0:T(1,128)} %bitcast.14, f32[128,3072]{1,0:T(8,128)} %gate_hbm.1, f32[128,3072]{1,0:T(8,128)} %up_hbm.1, f32[3072,128]{1,0:T(8,128)} %down_hbm.1, ...), custom_call_target="tpu_custom_call" | custom-call | tf_op jit(solution)/shard_map/pallas_call | solution.py:702
  248.8 1.9 copy.22

commit v5 on v4

--- a/solution.py
+++ b/solution.py
@@ -245,7 +245,7 @@
 
 
 EARLY = (
-    (4, QKV, 0), (5, QKV, 1), (9, QKV, 2), (11, QKV, 3), (12, OUT, 0), (12, OUT, 1), (13, OUT, 2), (13, OUT, 3),
+    (4, QKV, 0), (5, QKV, 1), (9, QKV, 2), (10, QKV, 3), (10, OUT, 0), (10, OUT, 1), (12, OUT, 2), (12, OUT, 3),
     (15, QKV, 4), (15, QKV, 5), (17, QKV, 6), (17, QKV, 7)
 )
 
@@ -463,7 +463,7 @@
                 v = (v * gain_ref[:, at]).astype(bf16)
                 acc[r, :columns] += jnp.dot(v, weights[at, :], preferred_element_type=f32)
 
-            row_tiles(seq, tile)
+            row_tiles(4 * seq, tile)
 
         return stage
 
@@ -484,16 +484,11 @@
                 [w_sc[pl.ds((base + h) * 8 + scale_row, 1), :] for h in (0, 1)], axis=1
             )
 
-            def step(i, _):
-                r = pl.ds(pl.multiple_of(i * 2 * seq, 2 * seq), 2 * seq)
-                term = jnp.dot(inputs[r, :], weights[:, at], preferred_element_type=f32) * factors
-                term = term.astype(bf16)
-                for m in range(2):
-                    for core in range(2):
-                        part[core, i * 2 + m, :, at] = term[(m * 2 + core) * own : (m * 2 + core + 1) * own]
-                return 0
-
-            lax.fori_loop(0, 2, step, 0)
+            term = jnp.dot(inputs[...], weights[:, at], preferred_element_type=f32) * factors
+            term = term.astype(bf16)
+            for m in range(4):
+                for core in range(2):
+                    part[core, m, :, at] = term[(m * 2 + core) * own : (m * 2 + core + 1) * own]
             to_twin(j).start()
 
         def to_twin(j):
@@ -613,7 +608,7 @@
     def first_gate(r):
         acc[r, :ff] = jnp.dot(rows_normed[r, :], w_gu[:, :ff], preferred_element_type=f32)
 
-    row_tiles(seq, first_gate)
+    row_tiles(2 * seq, first_gate)
     take_some(UP, 3, 4)
     pl.when(ahead)(lambda: send_far(QKV))
     pl.when(jnp.logical_not(ahead))(lambda: send_far(DN))
@@ -624,7 +619,7 @@
         up = jnp.dot(rows_normed[r, :], w_gu[:, ff:], preferred_element_type=f32)
         hidden[r, :] = silu_mul(acc[r, :ff], up)
 
-    row_tiles(seq, first_hidden)
+    row_tiles(2 * seq, first_hidden)
 
     def take_early(i):
         pl.when((i == 3) & ahead)(lambda: send_far(OUT))

time: 251 us -> 247 us (0.984)
  Pallas kernels: 249 us -> 245 us
    pallas_call x1, Pallas kernels: 249 us -> 245 us  [fused_body(): pl.pallas_call(fused_kernel, out_shape=jax.ShapeDtypeStruct((own, width),...]
where the time goes in v5:
time: 247 us
  Pallas kernels  245 us (99%)
    pallas_call x1, Pallas kernels, fused_body(): pl.pallas_call(fused_kernel, out_shape=jax.ShapeDtypeStruct((own, width),...  245 us

profile of v5, /device:TPU:0, one launch (start us, length us, event | category | flops | bytes accessed | tf_op | source)
XLA Modules:
  0.0 247.0 jit_solution(7483753770248666786)
XLA Ops:
  0.0 245.1 %shard_map.190 = bf16[128,2048]{1,0:T(8,128)(2,1)} custom-call(bf16[128,2048]{1,0:T(8,128)(2,1)} %res_ref.1, f32[1,2048]{1,0:T(1,128)} %bitcast.12, f32[1,2048]{1,0:T(1,128)} %bitcast.13, f32[1,2048]{1,0:T(1,128)} %bitcast.14, f32[128,3072]{1,0:T(8,128)} %gate_hbm.1, f32[128,3072]{1,0:T(8,128)} %up_hbm.1, f32[3072,128]{1,0:T(8,128)} %down_hbm.1, ...), custom_call_target="tpu_custom_call" | custom-call | tf_op jit(solution)/shard_map/pallas_call | solution.py:697
  245.1 1.9 copy.22

commit v6 on v5

--- a/solution.py
+++ b/solution.py
@@ -443,16 +443,12 @@
     def absorber(gain_ref, weights):
         columns = weights.shape[1]
 
+        def clear(r):
+            acc[r, :columns] = jnp.zeros((seq, columns), f32)
+            power[r, :] = jnp.zeros((seq, piece), f32)
+
         def stage(j):
             at = pl.ds(column(j), chunk)
-
-            @pl.when(j == 0)
-            def _():
-                def clear(r):
-                    acc[r, :columns] = jnp.zeros((seq, columns), f32)
-                    power[r, :] = jnp.zeros((seq, piece), f32)
-
-                row_tiles(seq, clear)
 
             ag_arrive(j)
 
@@ -465,7 +461,7 @@
 
             row_tiles(4 * seq, tile)
 
-        return stage
+        return stage, lambda: row_tiles(seq, clear)
 
     def row_factor(r):
         return lax.rsqrt(jnp.sum(power[r, :], axis=-1, keepdims=True) / width + EPSILON)
@@ -538,11 +534,13 @@
 
         stages = [product, reduce, relay, finish]
         if not last:
-            stages += [lambda j: ag_relay(j, rows), lambda j: ag_pass(j, rows), absorb]
+            stages += [lambda j: ag_relay(j, rows), lambda j: ag_pass(j, rows), absorb[0]]
 
         def step(i, _):
             for lag, stage in zip(lags, stages):
                 pl.when((i >= lag) & (i < chunks + lag))(lambda stage=stage, lag=lag: stage(i - lag))
+            if absorb is not None:
+                pl.when(i == 2)(absorb[1])
             if during is not None:
                 during(i)
             return 0
@@ -628,7 +626,7 @@
         for at, kind, j in EARLY:
             pl.when(i == at)(lambda kind=kind, j=j: take_pair(kind, j))
 
-    leave(hidden, w_d, 0, 0.5, DN, False, x_then_z, by_core, (0, 1, 4, 7, 9, 11, 12), absorber(g2_ref, w_qkv), take_early)
+    leave(hidden, w_d, 0, 0.5, DN, False, x_then_z, by_core, (0, 1, 4, 6, 9, 11, 12), absorber(g2_ref, w_qkv), take_early)
 
     take_some(OUT, 4, 8)
     head = (t * 4 + me).astype(f32)
@@ -663,7 +661,7 @@
         hidden[r, :] = silu_mul(acc[r, :ff] * factor, acc[r, ff : 2 * ff] * factor)
 
     row_tiles(own, second_hidden)
-    leave(hidden, w_d, 0, 0.5, None, True, by_core, by_core, (0, 1, 4, 8))
+    leave(hidden, w_d, 0, 0.5, None, True, by_core, by_core, (0, 1, 3, 7))
     for kind in (SC, GATE, UP, DN, QKV, OUT):
         finish_sends(kind)
 

time: 247 us -> 247 us (level)
  no operation moved by 1% of the time
where the time goes in v6:
time: 247 us; the launch traced here: 246 us
  Pallas kernels  244 us (99%)
    pallas_call x1, Pallas kernels, fused_body(): pl.pallas_call(fused_kernel, out_shape=jax.ShapeDtypeStruct((own, width),...  244 us

profile of v6, /device:TPU:0, one launch (start us, length us, event | category | flops | bytes accessed | tf_op | source)
XLA Modules:
  0.0 245.8 jit_solution(15675039575720462824)
XLA Ops:
  0.0 243.9 %shard_map.190 = bf16[128,2048]{1,0:T(8,128)(2,1)} custom-call(bf16[128,2048]{1,0:T(8,128)(2,1)} %res_ref.1, f32[1,2048]{1,0:T(1,128)} %bitcast.12, f32[1,2048]{1,0:T(1,128)} %bitcast.13, f32[1,2048]{1,0:T(1,128)} %bitcast.14, f32[128,3072]{1,0:T(8,128)} %gate_hbm.1, f32[128,3072]{1,0:T(8,128)} %up_hbm.1, f32[3072,128]{1,0:T(8,128)} %down_hbm.1, ...), custom_call_target="tpu_custom_call" | custom-call | tf_op jit(solution)/shard_map/pallas_call | solution.py:695
  244.0 1.9 copy.22
